TPU v7x, 32 devices: a whole 2x2x4 slice. The times are simulated.
32 devices in a mesh: sp: 8 (over z, x), tp: 4 (over y, core).
Axes of the slice: x: 2, y: 2, z: 4, core: 2. Of those that a mesh axis runs over, the one named last changes fastest.
Arguments:
- query_narrow: bfloat16 [2048, 1024], P('sp', 'tp'), may hold values from -6 to 6
- key_narrow: bfloat16 [2048, 1024], P('sp', 'tp'), may hold values from -6 to 6
- value_narrow: bfloat16 [2048, 1024], P('sp', 'tp'), may hold values from -12 to 12
- query_broad: bfloat16 [2048, 1024], P('sp', 'tp'), may hold values from -6 to 6
- key_broad: bfloat16 [2048, 1024], P('sp', 'tp'), may hold values from -6 to 6
- value_broad: bfloat16 [2048, 1024], P('sp', 'tp'), may hold values from -12 to 12
- offset_narrow: bfloat16 [16, 2048], P('tp', 'sp'), as said below
- offset_broad: bfloat16 [8, 2048], P('tp', 'sp'), as said below
- residual: bfloat16 [2048, 2048], P(('sp', 'tp')), may hold values from -6 to 6
- out_narrow: bfloat16 [1024, 2048], P('tp'), may hold values from -0.25 to 0.25
- out_broad: bfloat16 [1024, 2048], P('tp'), may hold values from -0.25 to 0.25
- norm_gain: float32 [2048], replicated, may hold values from 0.1 to 1.9
- up_proj: bfloat16 [2048, 8192], P('sp', 'tp'), may hold values from -0.125 to 0.125
- down_proj: bfloat16 [8192, 2048], P('tp', 'sp'), may hold values from -0.0625 to 0.0625
Outputs:
- output: bfloat16 [2048, 2048], P(('sp', 'tp'))
Inputs may be any that keep to these rules, and one draw needn't show every extreme that they name: `offset_narrow`: additive score offsets of each head for each key position. `offset_broad`: additive score offsets of each head for each key position.
All inputs are finite; a program needn't handle non-finite values.
Results may differ from a plain program's by a relative error of at most 0.018.
Values may be sent and summed in bfloat16 or wider, within the bound.
A program may use at most 64 MiB of HBM per device.

v0:
```python
import functools

import jax
import jax.numpy as jnp
from jax import lax
from jax.experimental import pallas as pl
from jax.experimental.pallas import tpu as pltpu
from jax.sharding import PartitionSpec as P

NARROW_SIZE = 64
BROAD_SIZE = 128
F32 = jnp.float32
BF16 = jnp.bfloat16


def ring_order(shards):
    across = 1 << ((shards.bit_length() - 1) // 2)
    along = shards // across
    order = [z * across for z in range(along)]
    for turn, z in enumerate(reversed(range(along))):
        row = list(range(1, across))
        if turn % 2:
            row.reverse()
        order += [z * across + x for x in row]
    return order


def lookup(table, index):
    found = jnp.int32(0)
    for place, value in enumerate(table):
        found = found + jnp.where(index == place, jnp.int32(value), jnp.int32(0))
    return found


def kernel(
    shards, peers, order,
    q_n, q_b, k_n, v_n, k_b, v_b, off_n, off_b, residual, out_n, out_b, gain, up, down,
    o_ref,
    kv_slots, off_slots, up_slots, down_slots, mixed, part, inbox, updated, normed_all,
    product, hidden, channel, send_sems, recv_sems, tp_send, tp_recv, load_sems,
):
    tok = q_n.shape[0]
    wide = product.shape[1]
    model = part.shape[2]
    rows = residual.shape[0]
    depth = up.shape[0]
    me = lax.axis_index("sp")
    me_tp = lax.axis_index("tp")
    inverse = [order.index(s) for s in range(shards)]
    pos = lookup(inverse, me)
    right = lookup(order, lax.rem(pos + 1, shards))
    left = lookup(order, lax.rem(pos + shards - 1, shards))

    half_up, half_down = wide // 2, wide // 2
    loads = []
    for way, (k, v, off) in enumerate(((k_n, v_n, off_n), (k_b, v_b, off_b))):
        loads += [
            (k, kv_slots.at[way, 0, pl.ds(0, tok)]),
            (v, kv_slots.at[way, 0, pl.ds(tok, tok)]),
            (off, off_slots.at[way, 0]),
        ]
    for way in range(2):
        loads += [
            (up.at[:, pl.ds(way * half_up, half_up)], up_slots.at[way, 0]),
            (down.at[pl.ds(way * half_down, half_down)], down_slots.at[way, 0]),
        ]
    loads = [
        pltpu.make_async_copy(src, dst, load_sems.at[i]) for i, (src, dst) in enumerate(loads)
    ]
    for load in loads:
        load.start()

    barrier = pltpu.get_barrier_semaphore()
    for shard in (left, right):
        pl.semaphore_signal(
            barrier, inc=1, device_id=(shard, me_tp), device_id_type=pl.DeviceIdType.MESH
        )
    for d in range(1, peers):
        pl.semaphore_signal(
            barrier, inc=1, device_id=(me, lax.rem(me_tp + d, peers)),
            device_id_type=pl.DeviceIdType.MESH,
        )
    pl.semaphore_wait(barrier, 1 + peers)

    def piece(stream, way, t):
        if stream == 0:
            return off_slots.at[way, t]
        if stream in (1, 2):
            return kv_slots.at[way, t, pl.ds((stream - 1) * tok, tok)]
        if stream in (3, 4):
            size = depth // 2
            return up_slots.at[way, t, pl.ds((stream - 3) * size, size)]
        size = half_down // 2
        return down_slots.at[way, t, pl.ds((stream - 5) * size, size)]

    def hop(stream, way, t):
        return pltpu.make_async_remote_copy(
            src_ref=piece(stream, way, t),
            dst_ref=piece(stream, way, t + 1),
            send_sem=send_sems.at[way, stream, t],
            recv_sem=recv_sems.at[way, stream, t],
            device_id=((left if way else right), me_tp),
            device_id_type=pl.DeviceIdType.MESH,
        )

    def begin(streams, t):
        for stream in streams:
            for way in range(2):
                hop(stream, way, t).start()

    def relay(streams, t):
        for stream in streams:
            for way in range(2):
                hop(stream, way, t - 1).wait_recv()
                hop(stream, way, t).start()

    def arrive(streams):
        for stream in streams:
            for way in range(2):
                hop(stream, way, shards - 2).wait_recv()

    def each(first, last, body):
        def step(t, carry):
            body(t)
            return carry

        lax.fori_loop(first, last, step, 0)

    KEYS, UPS, DOWNS = (0, 1, 2), (3, 4), (5, 6)
    for load in loads:
        load.wait()
    begin(KEYS, 0)
    each(1, shards - 1, functools.partial(relay, KEYS))
    begin(UPS, 0)
    arrive(KEYS)

    row_at = lax.broadcasted_iota(jnp.int32, (tok, tok), 0)
    col_at = lax.broadcasted_iota(jnp.int32, (tok, tok), 1)
    later = (row_at > col_at).astype(BF16)
    later2 = jnp.concatenate([later, later], axis=0)
    heads = []
    for way, (q, size) in enumerate(((q_n, NARROW_SIZE), (q_b, BROAD_SIZE))):
        for h in range(q.shape[1] // size):
            heads.append((way, h, size, q))

    def head_block(way, h, size, q, block, keep_sum, diagonal):
        there = lookup(inverse, block)
        slot = lax.rem((there - pos if way else pos - there) + shards, shards)
        cols = pl.ds(h * size, size)
        keys = kv_slots[way, slot, pl.ds(0, tok), cols]
        values = kv_slots[way, slot, pl.ds(tok, tok), cols]
        offset = off_slots[way, slot].astype(F32)[h : h + 1, :]
        scores = lax.dot_general(
            q[:, cols], keys, (((1,), (1,)), ((), ())), preferred_element_type=F32
        ) * (size ** -0.5) + offset
        keep = -(jnp.maximum(scores, 0.0) + jnp.log(1.0 + jnp.exp(-jnp.abs(scores))))
        breaks = scores + keep
        if diagonal:
            keep = jnp.where(col_at < row_at, keep, 0.0)
        high = keep.astype(BF16)
        low = (keep - high.astype(F32)).astype(BF16)
        after = jnp.dot(
            jnp.concatenate([high, low], axis=1), later2, preferred_element_type=F32
        )
        weight = jnp.exp(breaks + after + keep_sum)
        if diagonal:
            weight = jnp.where(col_at < row_at, weight, 0.0)
        added = jnp.dot(weight.astype(BF16), values, preferred_element_type=F32)
        return keep_sum + (after[:, :1] + keep[:, :1]), added

    turn_up = 1
    for index, (way, h, size, q) in enumerate(heads):
        start = head_block(way, h, size, q, me, jnp.zeros((tok, 1), F32), True)

        def sweep(turn, state, way=way, h=h, size=size, q=q):
            keep_sum, running = state
            keep_sum, added = head_block(way, h, size, q, me - 1 - turn, keep_sum, False)
            return keep_sum, running + added

        _, running = lax.fori_loop(0, me, sweep, start)
        base = way * q_n.shape[1] + h * size
        mixed[:, pl.ds(base, size)] = running.astype(BF16)
        if index % 2:
            relay(UPS, turn_up)
            turn_up += 1

    def tp_copy(src, dst, kind, d):
        return pltpu.make_async_remote_copy(
            src_ref=src, dst_ref=dst,
            send_sem=tp_send.at[kind, d - 1], recv_sem=tp_recv.at[kind, d - 1],
            device_id=(me, lax.rem(me_tp + d, peers)),
            device_id_type=pl.DeviceIdType.MESH,
        )

    def scatter(kind):
        copies = []
        for d in range(1, peers):
            peer = lax.rem(me_tp + d, peers)
            copies.append(
                tp_copy(
                    part.at[kind, pl.ds(pl.multiple_of(peer * rows, rows), rows)],
                    inbox.at[kind, d - 1], kind, d,
                )
            )
        for copy in copies:
            copy.start()
        return copies

    def summed(kind, copies):
        for copy in copies:
            copy.wait_recv()
        own = pl.multiple_of(me_tp * rows, rows)
        total = part[kind, pl.ds(own, rows), :].astype(F32)
        for d in range(1, peers):
            total = total + inbox[kind, d - 1].astype(F32)
        return total

    tile = min(512, model)
    n_cols = out_n.shape[0]

    def project(c):
        cols = pl.ds(pl.multiple_of(c * tile, tile), tile)
        part[0, :, cols] = (
            jnp.dot(mixed[:, :n_cols], out_n[:, cols], preferred_element_type=F32)
            + jnp.dot(mixed[:, n_cols:], out_b[:, cols], preferred_element_type=F32)
        ).astype(BF16)

    each(0, model // tile, project)
    first = scatter(0)
    relay(UPS, turn_up)
    updated[...] = residual[...].astype(F32) + summed(0, first)
    value = updated[...]
    scale = lax.rsqrt(jnp.mean(value * value, axis=-1, keepdims=True) + 1e-06)
    mine = pl.ds(pl.multiple_of(me_tp * rows, rows), rows)
    normed_all[mine, :] = (value * scale * gain[...]).astype(BF16)
    spread = [tp_copy(normed_all.at[mine], normed_all.at[mine], 2, d) for d in range(1, peers)]
    for copy in spread:
        copy.start()
    relay(UPS, turn_up + 1)
    for copy in spread:
        copy.wait_recv()

    product[...] = jnp.zeros_like(product)
    channel[...] = jnp.zeros_like(channel)
    step_cols = min(512, half_up)

    def source(way, t):
        return lookup(order, lax.rem((pos + t if way else pos - t + shards), shards))

    def climb(t):
        for way in range(2):
            lhs_cols = pl.ds(pl.multiple_of(source(way, t) * depth, depth), depth)

            def one(c, way=way, lhs_cols=lhs_cols):
                at = pl.multiple_of(c * step_cols, step_cols)
                product[:, pl.ds(way * half_up + at, step_cols)] += jnp.dot(
                    normed_all[:, lhs_cols], up_slots[way, t, :, pl.ds(at, step_cols)],
                    preferred_element_type=F32,
                )

            each(0, half_up // step_cols, one)

    def descend(t):
        for way in range(2):
            cols = pl.ds(pl.multiple_of(source(way, t) * depth, depth), depth)
            channel[:, cols] += jnp.dot(
                hidden[:, pl.ds(way * half_down, half_down)], down_slots[way, t],
                preferred_element_type=F32,
            )

    each(0, turn_up + 2, climb)

    def up_step(t):
        relay(UPS, t)
        climb(t)

    each(turn_up + 2, shards - 1, up_step)
    begin(DOWNS, 0)
    arrive(UPS)
    climb(shards - 1)

    def activate(c):
        cols = pl.ds(pl.multiple_of(c * step_cols, step_cols), step_cols)
        hidden[:, cols] = jnp.square(jnp.maximum(product[:, cols], 0.0)).astype(BF16)

    each(0, wide // step_cols, activate)
    descend(0)

    def down_step(t):
        relay(DOWNS, t)
        descend(t)

    each(1, shards - 1, down_step)
    arrive(DOWNS)
    descend(shards - 1)

    def settle(c):
        cols = pl.ds(pl.multiple_of(c * tile, tile), tile)
        part[1, :, cols] = channel[:, cols].astype(BF16)

    each(0, model // tile, settle)
    last = scatter(1)
    o_ref[...] = (updated[...] + summed(1, last)).astype(BF16)

    def drain(t):
        for stream in KEYS + UPS + DOWNS:
            for way in range(2):
                hop(stream, way, t).wait_send()

    each(0, shards - 1, drain)
    for copy in first + spread + last:
        copy.wait_send()


def local(
    shards, peers, order,
    query_narrow, key_narrow, value_narrow, query_broad, key_broad, value_broad,
    offset_narrow, offset_broad, residual, out_narrow, out_broad, norm_gain, up_proj, down_proj,
):
    tok, columns = query_narrow.shape
    rows, model = residual.shape
    depth, wide = up_proj.shape
    pad = 16

    def padded(offset):
        return jnp.pad(offset, ((0, pad - offset.shape[0]), (0, 0)))

    vmem = pl.BlockSpec(memory_space=pltpu.VMEM)
    anywhere = pl.BlockSpec(memory_space=pl.ANY)
    return pl.pallas_call(
        functools.partial(kernel, shards, peers, order),
        out_shape=jax.ShapeDtypeStruct((rows, model), BF16),
        in_specs=[vmem] * 2 + [anywhere] * 6 + [vmem] * 4 + [anywhere] * 2,
        out_specs=vmem,
        scratch_shapes=[
            pltpu.VMEM((2, shards, 2 * tok, columns), BF16),
            pltpu.VMEM((2, shards, pad, tok), BF16),
            pltpu.VMEM((2, shards, depth, wide // 2), BF16),
            pltpu.VMEM((2, shards, wide // 2, depth), BF16),
            pltpu.VMEM((tok, 2 * columns), BF16),
            pltpu.VMEM((2, tok, model), BF16),
            pltpu.VMEM((2, peers - 1, rows, model), BF16),
            pltpu.VMEM((rows, model), F32),
            pltpu.VMEM((tok, model), BF16),
            pltpu.VMEM((tok, wide), F32),
            pltpu.VMEM((tok, wide), BF16),
            pltpu.VMEM((tok, model), F32),
            pltpu.SemaphoreType.DMA((2, 7, shards)),
            pltpu.SemaphoreType.DMA((2, 7, shards)),
            pltpu.SemaphoreType.DMA((3, peers - 1)),
            pltpu.SemaphoreType.DMA((3, peers - 1)),
            pltpu.SemaphoreType.DMA((10,)),
        ],
        compiler_params=pltpu.CompilerParams(
            collective_id=0, has_side_effects=True, vmem_limit_bytes=60 << 20
        ),
    )(
        query_narrow, query_broad, key_narrow, value_narrow, key_broad, value_broad,
        padded(offset_narrow), padded(offset_broad), residual, out_narrow, out_broad,
        norm_gain.reshape(1, -1), up_proj, down_proj,
    )


def solution(mesh):
    shards, peers = mesh.shape["sp"], mesh.shape["tp"]
    return jax.shard_map(
        functools.partial(local, shards, peers, tuple(ring_order(shards))),
        mesh=mesh,
        in_specs=(
            P("sp", "tp"),
            P("sp", "tp"),
            P("sp", "tp"),
            P("sp", "tp"),
            P("sp", "tp"),
            P("sp", "tp"),
            P("tp", "sp"),
            P("tp", "sp"),
            P(("sp", "tp"), None),
            P("tp", None),
            P("tp", None),
            P(),
            P("sp", "tp"),
            P("tp", "sp"),
        ),
        out_specs=P(("sp", "tp"), None),
        check_vma=False,
    )
```

profile of v0, /device:TPU:0, one launch (start us, length us, event | category | flops | bytes accessed | tf_op | source)
XLA Modules:
  0.0 222.2 jit_solution(14054761730773502709)
XLA Ops:
  0.0 0.0 copy-start
  0.0 1.3 pad.8.off_n
  1.3 0.0 copy-done
  1.3 0.6 pad.9.off_b
  1.9 218.7 %shard_map.136 = bf16[64,2048]{1,0:T(8,128)(2,1)} custom-call(bf16[256,256]{1,0:T(8,128)(2,1)} %q_n.1, bf16[256,256]{1,0:T(8,128)(2,1)} %q_b.1, bf16[256,256]{1,0:T(8,128)(2,1)} %k_n.1, bf16[256,256]{1,0:T(8,128)(2,1)} %v_n.1, bf16[256,256]{1,0:T(8,128)(2,1)} %k_b.1, bf16[256,256]{1,0:T(8,128)(2,1)} %v_b.1, bf16[16,256]{1,0:T(8,128)(2,1)} %pad.8.off_n, ...), custom_call_target="tpu_custom_call" | custom-call | tf_op jit(solution)/shard_map/pallas_call | solution.py:330
  220.6 1.7 copy.16
Async XLA Ops:
  0.0 1.3 copy-start
where the time goes:
time: 226 us; the launch traced here: 222 us
  Pallas kernels  219 us (97%)
  local copies, waits for them, and re-layouts  3.57 us (2%)
    pallas_call x1, Pallas kernels, local(): pl.pallas_call(functools.partial(kernel, shards, peers, order), out_shape...  219 us

commit v1 on v0

v1 whole, which is shorter than its diff:
```python
import functools

import jax
import jax.numpy as jnp
from jax import lax
from jax.experimental import pallas as pl
from jax.experimental.pallas import tpu as pltpu
from jax.sharding import PartitionSpec as P

NARROW_SIZE = 64
BROAD_SIZE = 128
F32 = jnp.float32
BF16 = jnp.bfloat16


def ring_order(shards):
    across = 1 << ((shards.bit_length() - 1) // 2)
    along = shards // across
    order = [z * across for z in range(along)]
    for turn, z in enumerate(reversed(range(along))):
        row = list(range(1, across))
        if turn % 2:
            row.reverse()
        order += [z * across + x for x in row]
    return order


def lookup(table, index):
    found = jnp.int32(0)
    for place, value in enumerate(table):
        found = found + jnp.where(index == place, jnp.int32(value), jnp.int32(0))
    return found


def kernel(
    shards, peers, order, across, cores,
    q_n, q_b, k_n, v_n, k_b, v_b, off_n, off_b, residual, out_n, out_b, gain, up, down,
    o_ref,
    kv_slots, off_slots, up_src, down_src, up_buf, down_buf, mixed, part, inbox, updated,
    normed_all, hidden, channel, half_out, half_in, rows_out, rows_in,
    kv_send, kv_recv, a_send, a_recv, x_send, y_send, b_recv, tp_send, tp_recv,
    n_send, n_recv, h_send, h_recv, r_send, r_recv, load_sems,
):
    tok = q_n.shape[0]
    model = part.shape[1]
    rows = residual.shape[0]
    depth, wide = up.shape
    along, lanes = shards // across, peers // cores
    group = along * cores
    unit = wide // group
    me = lax.axis_index("sp")
    me_tp = lax.axis_index("tp")
    z, x = lax.div(me, across), lax.rem(me, across)
    y, c = lax.div(me_tp, cores), lax.rem(me_tp, cores)

    def turn(value, by, size):
        return lax.rem(value + by, size)

    def place(dz=0, dx=0, dy=0, dc=0):
        return (
            turn(z, dz, along) * across + turn(x, dx, across),
            turn(y, dy, lanes) * cores + turn(c, dc, cores),
        )

    def remote(src, dst, send_sem, recv_sem, where):
        return pltpu.make_async_remote_copy(
            src_ref=src, dst_ref=dst, send_sem=send_sem, recv_sem=recv_sem,
            device_id=where, device_id_type=pl.DeviceIdType.MESH,
        )

    started = []

    def launch(copy):
        copy.start()
        started.append(copy)

    inverse = [order.index(s) for s in range(shards)]
    pos = lookup(inverse, me)
    right = lookup(order, lax.rem(pos + 1, shards))
    left = lookup(order, lax.rem(pos + shards - 1, shards))

    def piece(m, shard, column):
        if m == 0:
            return up_buf.at[column, pl.ds(pl.multiple_of(shard * depth, depth), depth)]
        return down_buf.at[shard, pl.ds(pl.multiple_of(column * unit, unit), unit)]

    def block(m, shard, lane):
        if m == 0:
            return up_buf.at[
                pl.ds(lane * cores, cores), pl.ds(pl.multiple_of(shard * depth, depth), depth)
            ]
        size = cores * unit
        return down_buf.at[shard, pl.ds(pl.multiple_of(lane * size, size), size)]

    loads = []
    for way, (k, v, off) in enumerate(((k_n, v_n, off_n), (k_b, v_b, off_b))):
        loads += [
            (k, kv_slots.at[way, 0, pl.ds(0, tok)]),
            (v, kv_slots.at[way, 0, pl.ds(tok, tok)]),
            (off, off_slots.at[way, 0]),
        ]
    mine = pl.ds(pl.multiple_of((z * cores + c) * unit, unit), unit)
    weight_loads = [
        (up.at[:, pl.ds(j * unit, unit)], up_src.at[j]) for j in range(group)
    ] + [
        (down, down_src),
        (up.at[:, mine], piece(0, me, me_tp)),
        (down.at[mine], piece(1, me, me_tp)),
    ]
    loads = [
        pltpu.make_async_copy(src, dst, load_sems.at[i])
        for i, (src, dst) in enumerate(loads + weight_loads)
    ]
    for load in loads:
        load.start()
    weight_loads = loads[6:]
    loads = loads[:6]

    barrier = pltpu.get_barrier_semaphore()
    friends = [
        place(dz=dz, dc=dc) for dz in range(along) for dc in range(cores) if dz or dc
    ]
    friends += [place(dx=dx) for dx in range(1, across)]
    friends += [place(dy=dy, dc=dc) for dy in range(1, lanes) for dc in range(cores)]
    for friend in friends:
        pl.semaphore_signal(
            barrier, inc=1, device_id=friend, device_id_type=pl.DeviceIdType.MESH
        )
    pl.semaphore_wait(barrier, len(friends))

    def stream(kind, way, t):
        if kind == 0:
            return off_slots.at[way, t]
        return kv_slots.at[way, t, pl.ds((kind - 1) * tok, tok)]

    def hop(kind, way, t):
        return remote(
            stream(kind, way, t), stream(kind, way, t + 1),
            kv_send.at[way, kind, t], kv_recv.at[way, kind, t],
            ((left if way else right), me_tp),
        )

    def each(first, last, body):
        def step(t, carry):
            body(t)
            return carry

        lax.fori_loop(first, last, step, 0)

    def relay(t):
        for kind in range(3):
            for way in range(2):
                hop(kind, way, t - 1).wait_recv()
                hop(kind, way, t).start()

    def exchange(m, dz, dc):
        to = turn(z, dz, along) * cores + turn(c, dc, cores)
        if m == 0:
            src = up_src.at[to]
        else:
            src = down_src.at[pl.ds(pl.multiple_of(to * unit, unit), unit)]
        return remote(
            src, piece(m, me, me_tp), a_send.at[m, dz, dc], a_recv.at[m, dz, dc],
            place(dz=dz, dc=dc),
        )

    def send_column(m):
        for dz in range(along):
            for dc in range(cores):
                if dz or dc:
                    launch(exchange(m, dz, dc))

    def origin(dz, bx=0):
        return turn(z, along - dz, along) * across + turn(x, bx, across)

    def along_x(m, dz, by, dx):
        held = block(m, origin(dz), turn(y, by, lanes))
        return remote(
            held, held, x_send.at[m, dz, by, dx], b_recv.at[m, dz, (across - dx) % across, by],
            place(dx=dx),
        )

    def along_y(m, dz, bx, dy):
        held = block(m, origin(dz, bx), y)
        return remote(
            held, held, y_send.at[m, dz, bx, dy], b_recv.at[m, dz, bx, (lanes - dy) % lanes],
            place(dy=dy),
        )

    def await_block(m, dz, bx, by):
        held = block(m, origin(dz, bx), turn(y, by, lanes))
        remote(
            held, held, x_send.at[m, dz, 0, 0], b_recv.at[m, dz, bx, by], place(dc=1)
        ).wait_recv()

    def spread_block(m, dz):
        for dc in range(cores):
            if dz or dc:
                exchange(m, dz, dc).wait_recv()
        for dx in range(1, across):
            launch(along_x(m, dz, 0, dx))
        for dy in range(1, lanes):
            launch(along_y(m, dz, 0, dy))

    def relay_block(m, dz):
        if dz % 2 == 0:
            for bx in range(1, across):
                await_block(m, dz, bx, 0)
                for dy in range(1, lanes):
                    launch(along_y(m, dz, bx, dy))
        else:
            for by in range(1, lanes):
                await_block(m, dz, 0, by)
                for dx in range(1, across):
                    launch(along_x(m, dz, by, dx))

    def finish_weights(m):
        for dz in range(along):
            for bx in range(across):
                for by in range(lanes):
                    if bx and by or (by if dz % 2 == 0 else bx):
                        await_block(m, dz, bx, by)

    for load in loads:
        load.wait()
    for kind in range(3):
        for way in range(2):
            hop(kind, way, 0).start()
    for load in weight_loads:
        load.wait()
    each(1, shards - 1, relay)
    for kind in range(3):
        for way in range(2):
            hop(kind, way, shards - 2).wait_recv()

    send_column(0)
    send_column(1)
    spread_block(0, 0)
    spread_block(1, 0)

    row_at = lax.broadcasted_iota(jnp.int32, (tok, tok), 0)
    col_at = lax.broadcasted_iota(jnp.int32, (tok, tok), 1)
    later = (row_at > col_at).astype(BF16)
    later2 = jnp.concatenate([later, later], axis=0)
    heads = []
    for way, (q, size) in enumerate(((q_n, NARROW_SIZE), (q_b, BROAD_SIZE))):
        for h in range(q.shape[1] // size):
            heads.append((way, h, size, q))

    def head_block(way, h, size, q, at, keep_sum, diagonal):
        there = lookup(inverse, at)
        slot = lax.rem((there - pos if way else pos - there) + shards, shards)
        cols = pl.ds(h * size, size)
        keys = kv_slots[way, slot, pl.ds(0, tok), cols]
        values = kv_slots[way, slot, pl.ds(tok, tok), cols]
        offset = off_slots[way, slot].astype(F32)[h : h + 1, :]
        scores = lax.dot_general(
            q[:, cols], keys, (((1,), (1,)), ((), ())), preferred_element_type=F32
        ) * (size ** -0.5) + offset
        keep = -(jnp.maximum(scores, 0.0) + jnp.log(1.0 + jnp.exp(-jnp.abs(scores))))
        breaks = scores + keep
        if diagonal:
            keep = jnp.where(col_at < row_at, keep, 0.0)
        high = keep.astype(BF16)
        low = (keep - high.astype(F32)).astype(BF16)
        after = jnp.dot(
            jnp.concatenate([high, low], axis=1), later2, preferred_element_type=F32
        )
        weight = jnp.exp(breaks + after + keep_sum)
        if diagonal:
            weight = jnp.where(col_at < row_at, weight, 0.0)
        added = jnp.dot(weight.astype(BF16), values, preferred_element_type=F32)
        return keep_sum + (after[:, :1] + keep[:, :1]), added

    chores = []
    for dz in range(1, along):
        chores.append(functools.partial(spread_block, 0, dz))
        chores.append(functools.partial(relay_block, 0, dz - 1))
    for index, (way, h, size, q) in enumerate(heads):
        start = head_block(way, h, size, q, me, jnp.zeros((tok, 1), F32), True)

        def sweep(at, state, way=way, h=h, size=size, q=q):
            keep_sum, running = state
            keep_sum, added = head_block(way, h, size, q, me - 1 - at, keep_sum, False)
            return keep_sum, running + added

        _, running = lax.fori_loop(0, me, sweep, start)
        base = way * q_n.shape[1] + h * size
        mixed[:, pl.ds(base, size)] = running.astype(BF16)
        share = len(chores) * (index + 1) // len(heads) - len(chores) * index // len(heads)
        first_chore = len(chores) * index // len(heads)
        for chore in chores[first_chore : first_chore + share]:
            chore()

    tile = min(512, model)
    n_cols = out_n.shape[0]

    def project(i):
        cols = pl.ds(pl.multiple_of(i * tile, tile), tile)
        part[:, cols] = (
            jnp.dot(mixed[:, :n_cols], out_n[:, cols], preferred_element_type=F32)
            + jnp.dot(mixed[:, n_cols:], out_b[:, cols], preferred_element_type=F32)
        ).astype(BF16)

    each(0, model // tile, project)
    first = []
    for d in range(1, peers):
        peer = lax.rem(me_tp + d, peers)
        copy = remote(
            part.at[pl.ds(pl.multiple_of(peer * rows, rows), rows)], inbox.at[d - 1],
            tp_send.at[d - 1], tp_recv.at[d - 1], (me, peer),
        )
        launch(copy)
        first.append(copy)
    relay_block(0, along - 1)
    spread_block(1, 1)
    for copy in first:
        copy.wait_recv()
    total = part[pl.ds(pl.multiple_of(me_tp * rows, rows), rows), :].astype(F32)
    for d in range(1, peers):
        total = total + inbox[d - 1].astype(F32)
    updated[...] = residual[...].astype(F32) + total
    value = updated[...]
    scale = lax.rsqrt(jnp.mean(value * value, axis=-1, keepdims=True) + 1e-06)

    def rows_of(zz, cc):
        return pl.ds(pl.multiple_of((cc * along + zz) * rows, rows), rows)

    normed_all[rows_of(z, c), :] = (value * scale * gain[...]).astype(BF16)

    def pass_rows(dz, dc, via):
        held = normed_all.at[rows_of(turn(z, along - dz, along) if via else z, c)]
        return remote(
            held, held, n_send.at[dz, dc], n_recv.at[dz, dc],
            place(dc=dc) if via else place(dz=dz, dc=dc),
        )

    for dz in range(1, along):
        launch(pass_rows(dz, 0, False))
    for dc in range(1, cores):
        launch(pass_rows(0, dc, False))
    relay_block(1, 0)
    spread_block(1, 2)
    relay_block(1, 1)
    for dz in range(1, along):
        pass_rows(dz, 0, False).wait_recv()
        for dc in range(1, cores):
            launch(pass_rows(dz, dc, True))
    spread_block(1, 3) if along > 3 else None
    finish_weights(0)
    for dz in range(along):
        for dc in range(1, cores):
            pass_rows(dz, dc, dz > 0).wait_recv()

    def climb(i):
        product = jnp.dot(normed_all[...], up_buf[i], preferred_element_type=F32)
        cols = pl.ds(pl.multiple_of(i * unit, unit), unit)
        hidden[:, cols] = jnp.square(jnp.maximum(product, 0.0)).astype(BF16)

    each(0, peers, climb)
    for dz in range(2, along):
        relay_block(1, dz)
    finish_weights(1)

    own = along * rows
    chunks = 4
    width = model // chunks
    per = width // depth

    def halves(k, dc):
        cols = pl.ds(k * width, width)
        return remote(
            half_out.at[dc - 1, :, cols], half_in.at[dc - 1, :, cols],
            h_send.at[k, dc - 1], h_recv.at[k, dc - 1], place(dc=dc),
        )

    def sums(k, dz):
        cols = pl.ds(k * width, width)
        return remote(
            rows_out.at[dz - 1, :, cols], rows_in.at[dz - 1, :, cols],
            r_send.at[k, dz - 1], r_recv.at[k, dz - 1], place(dz=dz),
        )

    def gathered(zz, cols):
        found = channel[rows_of(zz, c), cols]
        at = pl.ds(pl.multiple_of(zz * rows, rows), rows)
        for dc in range(1, cores):
            found = found + half_in[dc - 1, at, cols].astype(F32)
        return found

    def descend(k):
        def one(s):
            cols = pl.ds(pl.multiple_of((k * per + s) * depth, depth), depth)
            channel[:, cols] = jnp.dot(
                hidden[...], down_buf[k * per + s], preferred_element_type=F32
            )

        each(0, per, one)
        cols = pl.ds(k * width, width)
        for dc in range(1, cores):
            theirs = pl.ds(pl.multiple_of(turn(c, dc, cores) * own, own), own)
            half_out[dc - 1, :, cols] = channel[theirs, cols].astype(BF16)
            launch(halves(k, dc))

    def hand_on(k):
        cols = pl.ds(k * width, width)
        for dc in range(1, cores):
            halves(k, dc).wait_recv()
        for dz in range(1, along):
            rows_out[dz - 1, :, cols] = gathered(turn(z, dz, along), cols).astype(BF16)
            launch(sums(k, dz))

    for k in range(chunks):
        descend(k)
        if k:
            hand_on(k - 1)
    hand_on(chunks - 1)
    for k in range(chunks):
        cols = pl.ds(k * width, width)
        total = updated[:, cols] + gathered(z, cols)
        for dz in range(1, along):
            sums(k, dz).wait_recv()
            total = total + rows_in[dz - 1, :, cols].astype(F32)
        o_ref[:, cols] = total.astype(BF16)

    def drain(t):
        for kind in range(3):
            for way in range(2):
                hop(kind, way, t).wait_send()

    each(0, shards - 1, drain)
    for copy in started:
        copy.wait_send()


def local(
    shards, peers, order, across, cores,
    query_narrow, key_narrow, value_narrow, query_broad, key_broad, value_broad,
    offset_narrow, offset_broad, residual, out_narrow, out_broad, norm_gain, up_proj, down_proj,
):
    tok, columns = query_narrow.shape
    rows, model = residual.shape
    depth, wide = up_proj.shape
    along, lanes = shards // across, peers // cores
    group = along * cores
    unit = wide // group
    chunks = 4
    pad = 16

    def padded(offset):
        return jnp.pad(offset, ((0, pad - offset.shape[0]), (0, 0)))

    vmem = pl.BlockSpec(memory_space=pltpu.VMEM)
    anywhere = pl.BlockSpec(memory_space=pl.ANY)
    dma = pltpu.SemaphoreType.DMA
    return pl.pallas_call(
        functools.partial(kernel, shards, peers, order, across, cores),
        out_shape=jax.ShapeDtypeStruct((rows, model), BF16),
        in_specs=[vmem] * 2 + [anywhere] * 6 + [vmem] * 4 + [anywhere] * 2,
        out_specs=vmem,
        scratch_shapes=[
            pltpu.VMEM((2, shards, 2 * tok, columns), BF16),
            pltpu.VMEM((2, shards, pad, tok), BF16),
            pltpu.VMEM((group, depth, unit), BF16),
            pltpu.VMEM((wide, depth), BF16),
            pltpu.VMEM((peers, model, unit), BF16),
            pltpu.VMEM((shards, peers * unit, depth), BF16),
            pltpu.VMEM((tok, 2 * columns), BF16),
            pltpu.VMEM((tok, model), BF16),
            pltpu.VMEM((peers - 1, rows, model), BF16),
            pltpu.VMEM((rows, model), F32),
            pltpu.VMEM((group * rows, model), BF16),
            pltpu.VMEM((group * rows, peers * unit), BF16),
            pltpu.VMEM((group * rows, model), F32),
            pltpu.VMEM((cores - 1, along * rows, model), BF16),
            pltpu.VMEM((cores - 1, along * rows, model), BF16),
            pltpu.VMEM((along - 1, rows, model), BF16),
            pltpu.VMEM((along - 1, rows, model), BF16),
            dma((2, 3, shards)),
            dma((2, 3, shards)),
            dma((2, along, cores)),
            dma((2, along, cores)),
            dma((2, along, lanes, across)),
            dma((2, along, across, lanes)),
            dma((2, along, across, lanes)),
            dma((peers - 1,)),
            dma((peers - 1,)),
            dma((along, cores)),
            dma((along, cores)),
            dma((chunks, cores)),
            dma((chunks, cores)),
            dma((chunks, along)),
            dma((chunks, along)),
            dma((group + 9,)),
        ],
        compiler_params=pltpu.CompilerParams(
            collective_id=0, has_side_effects=True, vmem_limit_bytes=60 << 20
        ),
    )(
        query_narrow, query_broad, key_narrow, value_narrow, key_broad, value_broad,
        padded(offset_narrow), padded(offset_broad), residual, out_narrow, out_broad,
        norm_gain.reshape(1, -1), up_proj, down_proj,
    )


def solution(mesh):
    shards, peers = mesh.shape["sp"], mesh.shape["tp"]
    across = 1 << ((shards.bit_length() - 1) // 2)
    return jax.shard_map(
        functools.partial(local, shards, peers, tuple(ring_order(shards)), across, 2),
        mesh=mesh,
        in_specs=(
            P("sp", "tp"),
            P("sp", "tp"),
            P("sp", "tp"),
            P("sp", "tp"),
            P("sp", "tp"),
            P("sp", "tp"),
            P("tp", "sp"),
            P("tp", "sp"),
            P(("sp", "tp"), None),
            P("tp", None),
            P("tp", None),
            P(),
            P("sp", "tp"),
            P("tp", "sp"),
        ),
        out_specs=P(("sp", "tp"), None),
        check_vma=False,
    )
```

time: 226 us -> 175 us (0.77); the launches traced: 222 us -> 174 us
  Pallas kernels: 219 us -> 171 us
    pallas_call x1, Pallas kernels: 219 us -> 171 us  [local(): pl.pallas_call(functools.partial(kernel, shards, peers, order, across, co...]
where the time goes in v1:
time: 175 us; the launch traced here: 174 us
  Pallas kernels  171 us (98%)
  local copies, waits for them, and re-layouts  3.57 us (2%)
    pallas_call x1, Pallas kernels, local(): pl.pallas_call(functools.partial(kernel, shards, peers, order, across, co...  171 us

profile of v1, /device:TPU:0, one launch (start us, length us, event | category | flops | bytes accessed | tf_op | source)
XLA Modules:
  0.0 174.4 jit_solution(1732370104596139229)
XLA Ops:
  0.0 0.0 copy-start
  0.0 1.3 pad.8.off_n
  1.3 0.0 copy-done
  1.3 0.6 pad.9.off_b
  1.9 170.8 %shard_map.136 = bf16[64,2048]{1,0:T(8,128)(2,1)} custom-call(bf16[256,256]{1,0:T(8,128)(2,1)} %q_n.1, bf16[256,256]{1,0:T(8,128)(2,1)} %q_b.1, bf16[256,256]{1,0:T(8,128)(2,1)} %k_n.1, bf16[256,256]{1,0:T(8,128)(2,1)} %v_n.1, bf16[256,256]{1,0:T(8,128)(2,1)} %k_b.1, bf16[256,256]{1,0:T(8,128)(2,1)} %v_b.1, bf16[16,256]{1,0:T(8,128)(2,1)} %pad.8.off_n, ...), custom_call_target="tpu_custom_call" | custom-call | tf_op jit(solution)/shard_map/pallas_call | solution.py:456
  172.7 1.7 copy.16
Async XLA Ops:
  0.0 1.3 copy-start

commit v2 on v1

--- a/solution.py
+++ b/solution.py
@@ -1,4 +1,5 @@
 import functools
+import math
 
 import jax
 import jax.numpy as jnp
@@ -11,6 +12,7 @@
 BROAD_SIZE = 128
 F32 = jnp.float32
 BF16 = jnp.bfloat16
+LOG2E = math.log2(math.e)
 
 
 def ring_order(shards):
@@ -33,13 +35,14 @@
 
 
 def kernel(
-    shards, peers, order, across, cores,
+    shards, peers, order, across, cores, column,
     q_n, q_b, k_n, v_n, k_b, v_b, off_n, off_b, residual, out_n, out_b, gain, up, down,
     o_ref,
-    kv_slots, off_slots, up_src, down_src, up_buf, down_buf, mixed, part, inbox, updated,
+    up_src, down_src, up_buf, down_buf, mixed, part, inbox, updated,
     normed_all, hidden, channel, half_out, half_in, rows_out, rows_in,
-    kv_send, kv_recv, a_send, a_recv, x_send, y_send, b_recv, tp_send, tp_recv,
-    n_send, n_recv, h_send, h_recv, r_send, r_recv, load_sems,
+    a_send, a_recv, x_send, y_send, b_recv, tp_send, tp_recv,
+    n_send, n_recv, h_send, h_recv, r_send, r_recv, load_sems, attention_sems,
+    *attention_scratch,
 ):
     tok = q_n.shape[0]
     model = part.shape[1]
@@ -74,11 +77,6 @@
         copy.start()
         started.append(copy)
 
-    inverse = [order.index(s) for s in range(shards)]
-    pos = lookup(inverse, me)
-    right = lookup(order, lax.rem(pos + 1, shards))
-    left = lookup(order, lax.rem(pos + shards - 1, shards))
-
     def piece(m, shard, column):
         if m == 0:
             return up_buf.at[column, pl.ds(pl.multiple_of(shard * depth, depth), depth)]
@@ -92,13 +90,6 @@
         size = cores * unit
         return down_buf.at[shard, pl.ds(pl.multiple_of(lane * size, size), size)]
 
-    loads = []
-    for way, (k, v, off) in enumerate(((k_n, v_n, off_n), (k_b, v_b, off_b))):
-        loads += [
-            (k, kv_slots.at[way, 0, pl.ds(0, tok)]),
-            (v, kv_slots.at[way, 0, pl.ds(tok, tok)]),
-            (off, off_slots.at[way, 0]),
-        ]
     mine = pl.ds(pl.multiple_of((z * cores + c) * unit, unit), unit)
     weight_loads = [
         (up.at[:, pl.ds(j * unit, unit)], up_src.at[j]) for j in range(group)
@@ -107,38 +98,33 @@
         (up.at[:, mine], piece(0, me, me_tp)),
         (down.at[mine], piece(1, me, me_tp)),
     ]
-    loads = [
+    weight_loads = [
         pltpu.make_async_copy(src, dst, load_sems.at[i])
-        for i, (src, dst) in enumerate(loads + weight_loads)
+        for i, (src, dst) in enumerate(weight_loads)
     ]
-    for load in loads:
-        load.start()
-    weight_loads = loads[6:]
-    loads = loads[:6]
-
-    barrier = pltpu.get_barrier_semaphore()
+
+    def begin(loads):
+        loads = [
+            pltpu.make_async_copy(src, dst, attention_sems.at[i])
+            for i, (src, dst) in enumerate(loads)
+        ]
+        for load in loads + weight_loads:
+            load.start()
+        return loads
+
     friends = [
         place(dz=dz, dc=dc) for dz in range(along) for dc in range(cores) if dz or dc
     ]
     friends += [place(dx=dx) for dx in range(1, across)]
     friends += [place(dy=dy, dc=dc) for dy in range(1, lanes) for dc in range(cores)]
-    for friend in friends:
-        pl.semaphore_signal(
-            barrier, inc=1, device_id=friend, device_id_type=pl.DeviceIdType.MESH
-        )
-    pl.semaphore_wait(barrier, len(friends))
-
-    def stream(kind, way, t):
-        if kind == 0:
-            return off_slots.at[way, t]
-        return kv_slots.at[way, t, pl.ds((kind - 1) * tok, tok)]
-
-    def hop(kind, way, t):
-        return remote(
-            stream(kind, way, t), stream(kind, way, t + 1),
-            kv_send.at[way, kind, t], kv_recv.at[way, kind, t],
-            ((left if way else right), me_tp),
-        )
+
+    def meet():
+        barrier = pltpu.get_barrier_semaphore()
+        for friend in friends:
+            pl.semaphore_signal(
+                barrier, inc=1, device_id=friend, device_id_type=pl.DeviceIdType.MESH
+            )
+        pl.semaphore_wait(barrier, len(friends))
 
     def each(first, last, body):
         def step(t, carry):
@@ -146,12 +132,6 @@
             return carry
 
         lax.fori_loop(first, last, step, 0)
-
-    def relay(t):
-        for kind in range(3):
-            for way in range(2):
-                hop(kind, way, t - 1).wait_recv()
-                hop(kind, way, t).start()
 
     def exchange(m, dz, dc):
         to = turn(z, dz, along) * cores + turn(c, dc, cores)
@@ -164,8 +144,8 @@
             place(dz=dz, dc=dc),
         )
 
-    def send_column(m):
-        for dz in range(along):
+    def send_column(m, hops):
+        for dz in hops:
             for dc in range(cores):
                 if dz or dc:
                     launch(exchange(m, dz, dc))
@@ -221,76 +201,347 @@
                     if bx and by or (by if dz % 2 == 0 else bx):
                         await_block(m, dz, bx, by)
 
-    for load in loads:
-        load.wait()
-    for kind in range(3):
-        for way in range(2):
-            hop(kind, way, 0).start()
-    for load in weight_loads:
-        load.wait()
-    each(1, shards - 1, relay)
-    for kind in range(3):
-        for way in range(2):
-            hop(kind, way, shards - 2).wait_recv()
-
-    send_column(0)
-    send_column(1)
-    spread_block(0, 0)
-    spread_block(1, 0)
-
+    everywhere = range(along)
+    beyond = range(1, along)
     row_at = lax.broadcasted_iota(jnp.int32, (tok, tok), 0)
     col_at = lax.broadcasted_iota(jnp.int32, (tok, tok), 1)
     later = (row_at > col_at).astype(BF16)
-    later2 = jnp.concatenate([later, later], axis=0)
-    heads = []
-    for way, (q, size) in enumerate(((q_n, NARROW_SIZE), (q_b, BROAD_SIZE))):
-        for h in range(q.shape[1] // size):
-            heads.append((way, h, size, q))
-
-    def head_block(way, h, size, q, at, keep_sum, diagonal):
-        there = lookup(inverse, at)
-        slot = lax.rem((there - pos if way else pos - there) + shards, shards)
-        cols = pl.ds(h * size, size)
-        keys = kv_slots[way, slot, pl.ds(0, tok), cols]
-        values = kv_slots[way, slot, pl.ds(tok, tok), cols]
-        offset = off_slots[way, slot].astype(F32)[h : h + 1, :]
-        scores = lax.dot_general(
-            q[:, cols], keys, (((1,), (1,)), ((), ())), preferred_element_type=F32
-        ) * (size ** -0.5) + offset
-        keep = -(jnp.maximum(scores, 0.0) + jnp.log(1.0 + jnp.exp(-jnp.abs(scores))))
-        breaks = scores + keep
+    before = col_at < row_at
+
+    def ring_attention():
+        kv_slots, off_slots, kv_send, kv_recv = attention_scratch
+        inverse = [order.index(s) for s in range(shards)]
+        pos = lookup(inverse, me)
+        right = lookup(order, lax.rem(pos + 1, shards))
+        left = lookup(order, lax.rem(pos + shards - 1, shards))
+        loads = []
+        for way, (k, v, off) in enumerate(((k_n, v_n, off_n), (k_b, v_b, off_b))):
+            loads += [
+                (k, kv_slots.at[way, 0, pl.ds(0, tok)]),
+                (v, kv_slots.at[way, 0, pl.ds(tok, tok)]),
+                (off, off_slots.at[way, 0]),
+            ]
+        loads = begin(loads)
+        meet()
+
+        def stream(kind, way, t):
+            if kind == 0:
+                return off_slots.at[way, t]
+            return kv_slots.at[way, t, pl.ds((kind - 1) * tok, tok)]
+
+        def hop(kind, way, t):
+            return remote(
+                stream(kind, way, t), stream(kind, way, t + 1),
+                kv_send.at[way, kind, t], kv_recv.at[way, kind, t],
+                ((left if way else right), me_tp),
+            )
+
+        def relay(t):
+            for kind in range(3):
+                for way in range(2):
+                    hop(kind, way, t - 1).wait_recv()
+                    hop(kind, way, t).start()
+
+        for load in loads:
+            load.wait()
+        for kind in range(3):
+            for way in range(2):
+                hop(kind, way, 0).start()
+        for load in weight_loads:
+            load.wait()
+        each(1, shards - 1, relay)
+        for kind in range(3):
+            for way in range(2):
+                hop(kind, way, shards - 2).wait_recv()
+        for m in range(2):
+            send_column(m, everywhere)
+        for m in range(2):
+            spread_block(m, 0)
+
+        def head_block(way, h, size, q, at, keep_sum, diagonal):
+            there = lookup(inverse, at)
+            slot = lax.rem((there - pos if way else pos - there) + shards, shards)
+            cols = pl.ds(h * size, size)
+            keys = kv_slots[way, slot, pl.ds(0, tok), cols]
+            values = kv_slots[way, slot, pl.ds(tok, tok), cols]
+            offset = off_slots[way, slot].astype(F32)[h : h + 1, :]
+            scores = lax.dot_general(
+                q[:, cols], keys, (((1,), (1,)), ((), ())), preferred_element_type=F32
+            ) * (size ** -0.5 * LOG2E) + offset * LOG2E
+            weight, spent = weigh(scores, diagonal, keep_sum)
+            added = jnp.dot(weight, values, preferred_element_type=F32)
+            return keep_sum + spent, added
+
+        for way, (q, size) in enumerate(((q_n, NARROW_SIZE), (q_b, BROAD_SIZE))):
+            for h in range(q.shape[1] // size):
+                start = head_block(way, h, size, q, me, jnp.zeros((tok, 1), F32), True)
+
+                def sweep(at, state, way=way, h=h, size=size, q=q):
+                    keep_sum, running = state
+                    keep_sum, added = head_block(
+                        way, h, size, q, me - 1 - at, keep_sum, False
+                    )
+                    return keep_sum, running + added
+
+                _, running = lax.fori_loop(0, me, sweep, start)
+                mixed[:, pl.ds(way * q.shape[1] + h * size, size)] = running.astype(BF16)
+        for dz in beyond:
+            spread_block(0, dz)
+
+        def drain(t):
+            for kind in range(3):
+                for way in range(2):
+                    hop(kind, way, t).wait_send()
+
+        return lambda: each(0, shards - 1, drain)
+
+    def weigh(scores, diagonal, spent_before=None):
+        spent = jnp.maximum(
+            scores, jnp.log2(1.0 + jnp.exp2(jnp.minimum(scores, 126.0)))
+        )
+        breaks = scores - spent
         if diagonal:
-            keep = jnp.where(col_at < row_at, keep, 0.0)
-        high = keep.astype(BF16)
-        low = (keep - high.astype(F32)).astype(BF16)
-        after = jnp.dot(
-            jnp.concatenate([high, low], axis=1), later2, preferred_element_type=F32
-        )
-        weight = jnp.exp(breaks + after + keep_sum)
+            spent = jnp.where(before, spent, 0.0)
+        rounded = spent.astype(BF16)
+        after = jnp.dot(rounded, later, preferred_element_type=F32)
+        power = breaks - after
+        if spent_before is not None:
+            power = power - spent_before
+        weight = jnp.exp2(power)
         if diagonal:
-            weight = jnp.where(col_at < row_at, weight, 0.0)
-        added = jnp.dot(weight.astype(BF16), values, preferred_element_type=F32)
-        return keep_sum + (after[:, :1] + keep[:, :1]), added
-
-    chores = []
-    for dz in range(1, along):
-        chores.append(functools.partial(spread_block, 0, dz))
-        chores.append(functools.partial(relay_block, 0, dz - 1))
-    for index, (way, h, size, q) in enumerate(heads):
-        start = head_block(way, h, size, q, me, jnp.zeros((tok, 1), F32), True)
-
-        def sweep(at, state, way=way, h=h, size=size, q=q):
-            keep_sum, running = state
-            keep_sum, added = head_block(way, h, size, q, me - 1 - at, keep_sum, False)
-            return keep_sum, running + added
-
-        _, running = lax.fori_loop(0, me, sweep, start)
-        base = way * q_n.shape[1] + h * size
-        mixed[:, pl.ds(base, size)] = running.astype(BF16)
-        share = len(chores) * (index + 1) // len(heads) - len(chores) * index // len(heads)
-        first_chore = len(chores) * index // len(heads)
-        for chore in chores[first_chore : first_chore + share]:
-            chore()
+            weight = jnp.where(before, weight, 0.0)
+        return weight.astype(BF16), after[:, :1] + rounded[:, :1].astype(F32)
+
+    def column_attention():
+        (
+            kv_src, q_src, kv_all, q_all, masked, running, spent, back,
+            kv_send, kv_recv, q_send, q_recv, over_send, over_recv, twin_send, twin_recv,
+            back_send, back_recv,
+        ) = attention_scratch
+        parts = along // cores
+        wide_part = q_src.shape[3]
+        row_parts = tok // wide_part
+        kinds = ((q_n, k_n, v_n, off_n, NARROW_SIZE), (q_b, k_b, v_b, off_b, BROAD_SIZE))
+        loads = []
+        for p in range(parts):
+            cols = pl.ds(p * wide_part, wide_part)
+            for kind, (q, k, v, _, _) in enumerate(kinds):
+                loads += [
+                    (k.at[:, cols], kv_src.at[p, kind, pl.ds(0, tok)]),
+                    (v.at[:, cols], kv_src.at[p, kind, pl.ds(tok, tok)]),
+                    (q.at[:, cols], q_src.at[p, kind]),
+                ]
+        loads = begin(loads)
+        pad = kv_src.shape[2] - 2 * tok
+        for p in range(parts):
+            for kind, (_, _, _, off, size) in enumerate(kinds):
+                per = wide_part // size
+                lines = []
+                for h in range(p * per, (p + 1) * per):
+                    for i in range(row_parts):
+                        lines.append(
+                            off[h : h + 1, pl.ds(i * wide_part, wide_part)].astype(F32)
+                        )
+                lines.append(jnp.zeros((pad - len(lines), wide_part), F32))
+                kv_src[p, kind, pl.ds(2 * tok, pad), :] = jnp.concatenate(
+                    lines, axis=0
+                ).astype(BF16)
+        meet()
+
+        source = lax.div(z, parts)
+        share = lax.rem(z, parts)
+        half = jnp.where(z >= cores, jnp.int32(1), jnp.int32(0))
+        taker = jnp.where(z >= cores, along - 1 - z, z)
+        shifted = []
+
+        def at_core(zz, core):
+            return (zz * across + x, y * cores + core)
+
+        def unless(same, copy):
+            @pl.when(jnp.logical_not(same))
+            def _():
+                copy.start()
+
+            shifted.append((same, copy))
+
+        for load in loads:
+            load.wait()
+        for p in range(parts):
+            zz = c * parts + p
+            for r in range(cores):
+                to = turn(c, r, cores)
+                same = jnp.logical_and(zz == z, to == c)
+                unless(same, remote(
+                    kv_src.at[p, to], kv_all.at[x, z, to], kv_send.at[p, r],
+                    kv_recv.at[z], at_core(zz, to),
+                ))
+
+                @pl.when(same)
+                def _(p=p, to=to):
+                    kv_all[x, z, to] = kv_src[p, to]
+
+            same = jnp.logical_and(zz == z, taker == c)
+            unless(same, remote(
+                q_src.at[p], q_all.at[half], q_send.at[p], q_recv.at[half],
+                at_core(zz, taker),
+            ))
+
+            @pl.when(same)
+            def _(p=p):
+                q_all[half] = q_src[p]
+
+        for load in weight_loads:
+            load.wait()
+        send_column(0, everywhere)
+        send_column(1, range(1))
+        spread_block(0, 0)
+
+        def from_z(dz):
+            return turn(z, along - dz, along)
+
+        def keys(bx, dz, core):
+            return kv_all.at[turn(x, bx, across), from_z(dz), core]
+
+        def await_keys(held, sem):
+            remote(held, held, kv_send.at[0, 0], sem, place(dc=1)).wait_recv()
+
+        def to_twin(bx, dz, dc):
+            held = keys(bx, dz, c)
+            launch(remote(
+                held, held, twin_send.at[bx, dz, dc], twin_recv.at[bx, dz, dc], place(dc=dc)
+            ))
+
+        for dz in everywhere:
+            if dz:
+                await_keys(keys(0, dz, c), kv_recv.at[from_z(dz)])
+            else:
+                @pl.when(source != c)
+                def _():
+                    await_keys(keys(0, 0, c), kv_recv.at[z])
+            held = keys(0, dz, c)
+            for dx in range(1, across):
+                launch(remote(
+                    held, held, over_send.at[dx, dz],
+                    over_recv.at[across - dx, dz], place(dx=dx),
+                ))
+            for dc in range(1, cores):
+                to_twin(0, dz, dc)
+        for bx in range(1, across):
+            for dz in everywhere:
+                await_keys(keys(bx, dz, c), over_recv.at[bx, dz])
+                for dc in range(1, cores):
+                    to_twin(bx, dz, dc)
+        spread_block(1, 0)
+        for bx in range(across):
+            for dz in everywhere:
+                for dc in range(1, cores):
+                    await_keys(
+                        keys(bx, dz, turn(c, cores - dc, cores)), twin_recv.at[bx, dz, dc]
+                    )
+
+        lane = lax.broadcasted_iota(jnp.int32, (tok, wide_part), 1)
+
+        def lanes_of(h, size):
+            return jnp.logical_and(lane >= h * size, lane < (h + 1) * size)
+
+        def block_of(bx, bz, diagonal):
+            scored = []
+            for kind, (_, _, _, _, size) in enumerate(kinds):
+                held = kv_all.at[bx, bz, kind]
+                lines = held[pl.ds(2 * tok, pad), :].astype(F32) * LOG2E
+                for h in range(wide_part // size):
+                    first = h * row_parts
+                    offset = jnp.concatenate(
+                        [lines[first + i : first + i + 1] for i in range(row_parts)], axis=1
+                    )
+                    scores = lax.dot_general(
+                        masked[kind, h], held[pl.ds(0, tok), :], (((1,), (1,)), ((), ())),
+                        preferred_element_type=F32,
+                    )
+                    scored.append((kind, h, scores * (size ** -0.5 * LOG2E) + offset))
+            weighed = [(kind, h, *weigh(scores, diagonal)) for kind, h, scores in scored]
+            for kind, (_, _, _, _, size) in enumerate(kinds):
+                values = kv_all[bx, bz, kind, pl.ds(tok, tok), :]
+                own = [(h, w, used) for which, h, w, used in weighed if which == kind]
+                added, total = None, None
+                for h, w, used in own:
+                    kept = values
+                    if len(own) > 1:
+                        kept = jnp.where(lanes_of(h, size), values, jnp.zeros_like(values))
+                    product = jnp.dot(w, kept, preferred_element_type=F32)
+                    used = jnp.broadcast_to(used, (tok, wide_part))
+                    added = product if added is None else added + product
+                    total = used if total is None else jnp.where(lanes_of(h, size), used, total)
+                if diagonal:
+                    running[kind] = added
+                    spent[kind] = total
+                else:
+                    running[kind] = running[kind] + added * jnp.exp2(-spent[kind])
+                    spent[kind] = spent[kind] + total
+
+        def sweep(zq, slot):
+            shard = zq * across + x
+            for kind, (_, _, _, _, size) in enumerate(kinds):
+                queries = q_all[slot, kind]
+                for h in range(wide_part // size):
+                    masked[kind, h] = jnp.where(
+                        lanes_of(h, size), queries, jnp.zeros_like(queries)
+                    )
+            block_of(x, zq, True)
+
+            def one(t):
+                at = shard - 1 - t
+                block_of(lax.rem(at, across), lax.div(at, across), False)
+
+            each(0, shard, one)
+            same = jnp.logical_and(zq == z, source == c)
+            for kind, (q, _, _, _, _) in enumerate(kinds):
+                at = kind * q.shape[1] + share * wide_part
+                cols = pl.ds(pl.multiple_of(at, wide_part), wide_part)
+                back[slot, kind] = running[kind].astype(BF16)
+                unless(same, remote(
+                    back.at[slot, kind], mixed.at[:, cols], back_send.at[slot, kind],
+                    back_recv.at[share, kind], at_core(zq, source),
+                ))
+
+                @pl.when(same)
+                def _(kind=kind, cols=cols):
+                    mixed[:, cols] = running[kind].astype(BF16)
+
+        for slot in range(2):
+            zq = c if slot == 0 else along - 1 - c
+
+            @pl.when(jnp.logical_not(jnp.logical_and(zq == z, source == c)))
+            def _(slot=slot):
+                remote(
+                    q_all.at[slot], q_all.at[slot], q_send.at[0], q_recv.at[slot], place(dc=1)
+                ).wait_recv()
+
+            sweep(zq, slot)
+            relay_block(slot, 0)
+        send_column(1, beyond)
+        for dz in beyond:
+            spread_block(0, dz)
+        for p in range(parts):
+            same = jnp.logical_and(c * parts + p == z, taker == c)
+
+            @pl.when(jnp.logical_not(same))
+            def _(p=p):
+                for kind, (q, _, _, _, _) in enumerate(kinds):
+                    held = mixed.at[:, pl.ds(kind * q.shape[1] + p * wide_part, wide_part)]
+                    remote(
+                        held, held, back_send.at[0, 0], back_recv.at[p, kind], place(dc=1)
+                    ).wait_recv()
+
+        def drain():
+            for same, copy in shifted:
+                @pl.when(jnp.logical_not(same))
+                def _(copy=copy):
+                    copy.wait_send()
+
+        return drain
+
+    drain = column_attention() if column else ring_attention()
 
     tile = min(512, model)
     n_cols = out_n.shape[0]
@@ -312,8 +563,8 @@
         )
         launch(copy)
         first.append(copy)
-    relay_block(0, along - 1)
-    spread_block(1, 1)
+    for dz in range(0 if not column else 1, along):
+        relay_block(0, dz)
     for copy in first:
         copy.wait_recv()
     total = part[pl.ds(pl.multiple_of(me_tp * rows, rows), rows), :].astype(F32)
@@ -339,14 +590,14 @@
         launch(pass_rows(dz, 0, False))
     for dc in range(1, cores):
         launch(pass_rows(0, dc, False))
-    relay_block(1, 0)
-    spread_block(1, 2)
-    relay_block(1, 1)
+    if not column:
+        relay_block(1, 0)
+    for dz in beyond:
+        spread_block(1, dz)
     for dz in range(1, along):
         pass_rows(dz, 0, False).wait_recv()
         for dc in range(1, cores):
             launch(pass_rows(dz, dc, True))
-    spread_block(1, 3) if along > 3 else None
     finish_weights(0)
     for dz in range(along):
         for dc in range(1, cores):
@@ -358,7 +609,7 @@
         hidden[:, cols] = jnp.square(jnp.maximum(product, 0.0)).astype(BF16)
 
     each(0, peers, climb)
-    for dz in range(2, along):
+    for dz in beyond:
         relay_block(1, dz)
     finish_weights(1)
 
@@ -423,12 +674,7 @@
             total = total + rows_in[dz - 1, :, cols].astype(F32)
         o_ref[:, cols] = total.astype(BF16)
 
-    def drain(t):
-        for kind in range(3):
-            for way in range(2):
-                hop(kind, way, t).wait_send()
-
-    each(0, shards - 1, drain)
+    drain()
     for copy in started:
         copy.wait_send()
 
@@ -446,21 +692,60 @@
     unit = wide // group
     chunks = 4
     pad = 16
+    parts = max(1, along // cores)
+    part_columns = columns // parts
+    column = (
+        along == 2 * cores
+        and columns % parts == 0
+        and part_columns % BROAD_SIZE == 0
+        and tok % part_columns == 0
+    )
 
     def padded(offset):
+        if column:
+            return offset
         return jnp.pad(offset, ((0, pad - offset.shape[0]), (0, 0)))
 
     vmem = pl.BlockSpec(memory_space=pltpu.VMEM)
     anywhere = pl.BlockSpec(memory_space=pl.ANY)
     dma = pltpu.SemaphoreType.DMA
+    if column:
+        span = 2 * tok + pad
+        in_specs = [anywhere] * 6 + [vmem] * 6 + [anywhere] * 2
+        attention_scratch = [
+            pltpu.VMEM((parts, 2, span, part_columns), BF16),
+            pltpu.VMEM((parts, 2, tok, part_columns), BF16),
+            pltpu.VMEM((across, along, 2, span, part_columns), BF16),
+            pltpu.VMEM((2, 2, tok, part_columns), BF16),
+            pltpu.VMEM((2, part_columns // NARROW_SIZE, tok, part_columns), BF16),
+            pltpu.VMEM((2, tok, part_columns), F32),
+            pltpu.VMEM((2, tok, part_columns), F32),
+            pltpu.VMEM((2, 2, tok, part_columns), BF16),
+            dma((parts, cores)),
+            dma((along,)),
+            dma((parts,)),
+            dma((2,)),
+            dma((across, along)),
+            dma((across, along)),
+            dma((across, along, cores)),
+            dma((across, along, cores)),
+            dma((2, 2)),
+            dma((parts, 2)),
+        ]
+    else:
+        in_specs = [vmem] * 2 + [anywhere] * 6 + [vmem] * 4 + [anywhere] * 2
+        attention_scratch = [
+            pltpu.VMEM((2, shards, 2 * tok, columns), BF16),
+            pltpu.VMEM((2, shards, pad, tok), BF16),
+            dma((2, 3, shards)),
+            dma((2, 3, shards)),
+        ]
     return pl.pallas_call(
-        functools.partial(kernel, shards, peers, order, across, cores),
+        functools.partial(kernel, shards, peers, order, across, cores, column),
         out_shape=jax.ShapeDtypeStruct((rows, model), BF16),
-        in_specs=[vmem] * 2 + [anywhere] * 6 + [vmem] * 4 + [anywhere] * 2,
+        in_specs=in_specs,
         out_specs=vmem,
         scratch_shapes=[
-            pltpu.VMEM((2, shards, 2 * tok, columns), BF16),
-            pltpu.VMEM((2, shards, pad, tok), BF16),
             pltpu.VMEM((group, depth, unit), BF16),
             pltpu.VMEM((wide, depth), BF16),
             pltpu.VMEM((peers, model, unit), BF16),
@@ -476,8 +761,6 @@
             pltpu.VMEM((cores - 1, along * rows, model), BF16),
             pltpu.VMEM((along - 1, rows, model), BF16),
             pltpu.VMEM((along - 1, rows, model), BF16),
-            dma((2, 3, shards)),
-            dma((2, 3, shards)),
             dma((2, along, cores)),
             dma((2, along, cores)),
             dma((2, along, lanes, across)),
@@ -491,8 +774,9 @@
             dma((chunks, cores)),
             dma((chunks, along)),
             dma((chunks, along)),
-            dma((group + 9,)),
-        ],
+            dma((group + 3,)),
+            dma((6 * max(parts, 1),)),
+        ] + attention_scratch,
         compiler_params=pltpu.CompilerParams(
             collective_id=0, has_side_effects=True, vmem_limit_bytes=60 << 20
         ),

time: 175 us -> 155 us (0.89)
  Pallas kernels: 171 us -> 153 us
  local copies, waits for them, and re-layouts: 3.57 us -> 1.67 us
    pallas_call x1, Pallas kernels: 171 us -> 153 us  [local(): pl.pallas_call(functools.partial(kernel, shards, peers, order, across, co...]
    pad x2 -> x0, local copies, waits for them, and re-layouts: 1.9 us -> none  [padded(): return jnp.pad(offset, ((0, pad - offset.shape[0]), (0, 0)))]
where the time goes in v2:
time: 155 us; the launch traced here: 154 us
  Pallas kernels  153 us (99%)
  local copies, waits for them, and re-layouts  1.67 us (1%)
    pallas_call x1, Pallas kernels, local(): pl.pallas_call(functools.partial(kernel, shards, peers, order, across, co...  153 us

profile of v2, /device:TPU:0, one launch (start us, length us, event | category | flops | bytes accessed | tf_op | source)
XLA Modules:
  0.0 154.4 jit_solution(2136033986681568318)
XLA Ops:
  0.0 152.7 %shard_map.136 = bf16[64,2048]{1,0:T(8,128)(2,1)} custom-call(bf16[256,256]{1,0:T(8,128)(2,1)} %q_n.1, bf16[256,256]{1,0:T(8,128)(2,1)} %q_b.1, bf16[256,256]{1,0:T(8,128)(2,1)} %k_n.1, bf16[256,256]{1,0:T(8,128)(2,1)} %v_n.1, bf16[256,256]{1,0:T(8,128)(2,1)} %k_b.1, bf16[256,256]{1,0:T(8,128)(2,1)} %v_b.1, bf16[4,256]{1,0:T(4,128)(2,1)} %off_n.1, ...), custom_call_target="tpu_custom_call" | custom-call | tf_op jit(solution)/shard_map/pallas_call | solution.py:743
  152.7 1.7 %copy.16 = bf16[64,2048]{1,0:T(8,128)(2,1)} copy(bf16[64,2048]{1,0:T(8,128)(2,1)} %shard_map.136) | data formatting | bytes 524288

commit v3 on v2

--- a/solution.py
+++ b/solution.py
@@ -38,10 +38,11 @@
     shards, peers, order, across, cores, column,
     q_n, q_b, k_n, v_n, k_b, v_b, off_n, off_b, residual, out_n, out_b, gain, up, down,
     o_ref,
-    up_src, down_src, up_buf, down_buf, mixed, part, inbox, updated,
+    up_src, down_src, up_buf, down_buf, out_all, mixed, part, twin_out, twin_in,
+    lane_out, lane_in, updated,
     normed_all, hidden, channel, half_out, half_in, rows_out, rows_in,
-    a_send, a_recv, x_send, y_send, b_recv, tp_send, tp_recv,
-    n_send, n_recv, h_send, h_recv, r_send, r_recv, load_sems, attention_sems,
+    a_send, a_recv, x_send, y_send, b_recv, t_send, t_recv, l_send, l_recv,
+    n_send, n_recv, w_send, w_recv, h_send, h_recv, r_send, r_recv, load_sems, attention_sems,
     *attention_scratch,
 ):
     tok = q_n.shape[0]
@@ -82,14 +83,8 @@
             return up_buf.at[column, pl.ds(pl.multiple_of(shard * depth, depth), depth)]
         return down_buf.at[shard, pl.ds(pl.multiple_of(column * unit, unit), unit)]
 
-    def block(m, shard, lane):
-        if m == 0:
-            return up_buf.at[
-                pl.ds(lane * cores, cores), pl.ds(pl.multiple_of(shard * depth, depth), depth)
-            ]
-        size = cores * unit
-        return down_buf.at[shard, pl.ds(pl.multiple_of(lane * size, size), size)]
-
+    far_first = sorted(range(1, along), key=lambda dz: abs(2 * dz - along))
+    columns = out_n.shape[0]
     mine = pl.ds(pl.multiple_of((z * cores + c) * unit, unit), unit)
     weight_loads = [
         (up.at[:, pl.ds(j * unit, unit)], up_src.at[j]) for j in range(group)
@@ -97,6 +92,8 @@
         (down, down_src),
         (up.at[:, mine], piece(0, me, me_tp)),
         (down.at[mine], piece(1, me, me_tp)),
+        (out_n, out_all.at[pl.ds(0, columns)]),
+        (out_b, out_all.at[pl.ds(columns, columns)]),
     ]
     weight_loads = [
         pltpu.make_async_copy(src, dst, load_sems.at[i])
@@ -153,53 +150,70 @@
     def origin(dz, bx=0):
         return turn(z, along - dz, along) * across + turn(x, bx, across)
 
-    def along_x(m, dz, by, dx):
-        held = block(m, origin(dz), turn(y, by, lanes))
+    def part_of(m, dz, dc, bx, by):
+        core = turn(c, cores - dc, cores)
+        return piece(m, origin(dz, bx), turn(y, by, lanes) * cores + core)
+
+    def along_x(m, dz, dc, by, dx):
+        held = part_of(m, dz, dc, 0, by)
         return remote(
-            held, held, x_send.at[m, dz, by, dx], b_recv.at[m, dz, (across - dx) % across, by],
-            place(dx=dx),
-        )
-
-    def along_y(m, dz, bx, dy):
-        held = block(m, origin(dz, bx), y)
+            held, held, x_send.at[m, dz, dc, by, dx],
+            b_recv.at[m, dz, dc, (across - dx) % across, by], place(dx=dx),
+        )
+
+    def along_y(m, dz, dc, bx, dy):
+        held = part_of(m, dz, dc, bx, 0)
         return remote(
-            held, held, y_send.at[m, dz, bx, dy], b_recv.at[m, dz, bx, (lanes - dy) % lanes],
-            place(dy=dy),
-        )
-
-    def await_block(m, dz, bx, by):
-        held = block(m, origin(dz, bx), turn(y, by, lanes))
+            held, held, y_send.at[m, dz, dc, bx, dy],
+            b_recv.at[m, dz, dc, bx, (lanes - dy) % lanes], place(dy=dy),
+        )
+
+    def await_part(m, dz, dc, bx, by):
+        held = part_of(m, dz, dc, bx, by)
         remote(
-            held, held, x_send.at[m, dz, 0, 0], b_recv.at[m, dz, bx, by], place(dc=1)
+            held, held, x_send.at[m, dz, dc, 0, 0], b_recv.at[m, dz, dc, bx, by], place(dc=1)
         ).wait_recv()
 
-    def spread_block(m, dz):
-        for dc in range(cores):
+    arrived = set()
+
+    def spread_part(m, dz, dc, x_too=True, y_too=True):
+        if (m, dz, dc) not in arrived:
+            arrived.add((m, dz, dc))
             if dz or dc:
                 exchange(m, dz, dc).wait_recv()
-        for dx in range(1, across):
-            launch(along_x(m, dz, 0, dx))
-        for dy in range(1, lanes):
-            launch(along_y(m, dz, 0, dy))
+        if x_too:
+            for dx in range(1, across):
+                launch(along_x(m, dz, dc, 0, dx))
+        if y_too:
+            for dy in range(1, lanes):
+                launch(along_y(m, dz, dc, 0, dy))
+
+    def spread_block(m, dz, x_too=True, y_too=True):
+        for dc in range(cores):
+            spread_part(m, dz, dc, x_too, y_too)
+
+    def x_first(dz, dc):
+        return (dz + dc) % 2 == 0
 
     def relay_block(m, dz):
-        if dz % 2 == 0:
-            for bx in range(1, across):
-                await_block(m, dz, bx, 0)
-                for dy in range(1, lanes):
-                    launch(along_y(m, dz, bx, dy))
-        else:
-            for by in range(1, lanes):
-                await_block(m, dz, 0, by)
-                for dx in range(1, across):
-                    launch(along_x(m, dz, by, dx))
-
-    def finish_weights(m):
-        for dz in range(along):
+        for dc in range(cores):
+            if x_first(dz, dc):
+                for bx in range(1, across):
+                    await_part(m, dz, dc, bx, 0)
+                    for dy in range(1, lanes):
+                        launch(along_y(m, dz, dc, bx, dy))
+            else:
+                for by in range(1, lanes):
+                    await_part(m, dz, dc, 0, by)
+                    for dx in range(1, across):
+                        launch(along_x(m, dz, dc, by, dx))
+
+    def finish_block(m, dz):
+        for dc in range(cores):
             for bx in range(across):
                 for by in range(lanes):
-                    if bx and by or (by if dz % 2 == 0 else bx):
-                        await_block(m, dz, bx, by)
+                    if bx and by or (by if x_first(dz, dc) else bx):
+                        await_part(m, dz, dc, bx, by)
 
     everywhere = range(along)
     beyond = range(1, along)
@@ -254,7 +268,8 @@
             for way in range(2):
                 hop(kind, way, shards - 2).wait_recv()
         for m in range(2):
-            send_column(m, everywhere)
+            send_column(m, range(1))
+        send_column(0, beyond)
         for m in range(2):
             spread_block(m, 0)
 
@@ -285,7 +300,7 @@
 
                 _, running = lax.fori_loop(0, me, sweep, start)
                 mixed[:, pl.ds(way * q.shape[1] + h * size, size)] = running.astype(BF16)
-        for dz in beyond:
+        for dz in far_first[:1]:
             spread_block(0, dz)
 
         def drain(t):
@@ -392,7 +407,7 @@
 
         for load in weight_loads:
             load.wait()
-        send_column(0, everywhere)
+        send_column(0, range(1))
         send_column(1, range(1))
         spread_block(0, 0)
 
@@ -426,6 +441,7 @@
                 ))
             for dc in range(1, cores):
                 to_twin(0, dz, dc)
+        send_column(0, far_first[:1])
         for bx in range(1, across):
             for dz in everywhere:
                 await_keys(keys(bx, dz, c), over_recv.at[bx, dz])
@@ -519,8 +535,8 @@
 
             sweep(zq, slot)
             relay_block(slot, 0)
-        send_column(1, beyond)
-        for dz in beyond:
+        send_column(0, far_first[1:2])
+        for dz in far_first[:1]:
             spread_block(0, dz)
         for p in range(parts):
             same = jnp.logical_and(c * parts + p == z, taker == c)
@@ -533,6 +549,9 @@
                         held, held, back_send.at[0, 0], back_recv.at[p, kind], place(dc=1)
                     ).wait_recv()
 
+        send_column(0, far_first[2:])
+        send_column(1, far_first[:1])
+
         def drain():
             for same, copy in shifted:
                 @pl.when(jnp.logical_not(same))
@@ -543,34 +562,63 @@
 
     drain = column_attention() if column else ring_attention()
 
-    tile = min(512, model)
-    n_cols = out_n.shape[0]
-
-    def project(i):
-        cols = pl.ds(pl.multiple_of(i * tile, tile), tile)
-        part[:, cols] = (
-            jnp.dot(mixed[:, :n_cols], out_n[:, cols], preferred_element_type=F32)
-            + jnp.dot(mixed[:, n_cols:], out_b[:, cols], preferred_element_type=F32)
-        ).astype(BF16)
-
-    each(0, model // tile, project)
-    first = []
-    for d in range(1, peers):
-        peer = lax.rem(me_tp + d, peers)
-        copy = remote(
-            part.at[pl.ds(pl.multiple_of(peer * rows, rows), rows)], inbox.at[d - 1],
-            tp_send.at[d - 1], tp_recv.at[d - 1], (me, peer),
-        )
-        launch(copy)
-        first.append(copy)
-    for dz in range(0 if not column else 1, along):
+    chunks = 4
+    width = model // chunks
+
+    def chunk(k):
+        return pl.ds(k * width, width)
+
+    def twins(k, dc):
+        return remote(
+            twin_out.at[dc - 1, :, chunk(k)], twin_in.at[dc - 1, :, chunk(k)],
+            t_send.at[k, dc - 1], t_recv.at[k, dc - 1], place(dc=dc),
+        )
+
+    def others(k, dy):
+        return remote(
+            lane_out.at[dy - 1, :, chunk(k)], lane_in.at[dy - 1, :, chunk(k)],
+            l_send.at[k, dy - 1], l_recv.at[k, dy - 1], place(dy=dy),
+        )
+
+    def part_rows(lane, core):
+        return pl.ds(pl.multiple_of((lane * cores + core) * rows, rows), rows)
+
+    def paired(lane, k):
+        found = part[part_rows(lane, c), chunk(k)]
+        at = pl.ds(pl.multiple_of(lane * rows, rows), rows)
+        for dc in range(1, cores):
+            found = found + twin_in[dc - 1, at, chunk(k)].astype(F32)
+        return found
+
+    for k in range(chunks):
+        part[:, chunk(k)] = jnp.dot(
+            mixed[...], out_all[:, chunk(k)], preferred_element_type=F32
+        )
+        for dc in range(1, cores):
+            for lane in range(lanes):
+                twin_out[dc - 1, pl.ds(lane * rows, rows), chunk(k)] = part[
+                    part_rows(lane, turn(c, dc, cores)), chunk(k)
+                ].astype(BF16)
+            launch(twins(k, dc))
+    for k in range(chunks):
+        for dc in range(1, cores):
+            twins(k, dc).wait_recv()
+        for dy in range(1, lanes):
+            lane_out[dy - 1, :, chunk(k)] = paired(turn(y, dy, lanes), k).astype(BF16)
+            launch(others(k, dy))
+    if not column:
+        relay_block(0, 0)
+        relay_block(1, 0)
+    for dz in far_first[:1]:
         relay_block(0, dz)
-    for copy in first:
-        copy.wait_recv()
-    total = part[pl.ds(pl.multiple_of(me_tp * rows, rows), rows), :].astype(F32)
-    for d in range(1, peers):
-        total = total + inbox[d - 1].astype(F32)
-    updated[...] = residual[...].astype(F32) + total
+    for dz in far_first[1:2]:
+        spread_block(0, dz, y_too=False)
+    for k in range(chunks):
+        total = residual[:, chunk(k)].astype(F32) + paired(y, k)
+        for dy in range(1, lanes):
+            others(k, dy).wait_recv()
+            total = total + lane_in[dy - 1, :, chunk(k)].astype(F32)
+        updated[:, chunk(k)] = total
     value = updated[...]
     scale = lax.rsqrt(jnp.mean(value * value, axis=-1, keepdims=True) + 1e-06)
 
@@ -579,29 +627,75 @@
 
     normed_all[rows_of(z, c), :] = (value * scale * gain[...]).astype(BF16)
 
-    def pass_rows(dz, dc, via):
-        held = normed_all.at[rows_of(turn(z, along - dz, along) if via else z, c)]
+    def rows_at(zz):
+        return normed_all.at[rows_of(zz, c)]
+
+    def pass_line(zz, way, step):
+        to = z + (-1 if way else 1)
         return remote(
-            held, held, n_send.at[dz, dc], n_recv.at[dz, dc],
-            place(dc=dc) if via else place(dz=dz, dc=dc),
-        )
-
-    for dz in range(1, along):
-        launch(pass_rows(dz, 0, False))
+            rows_at(zz), rows_at(zz), n_send.at[way, step], n_recv.at[way, step],
+            (to * across + x, me_tp),
+        )
+
+    def pass_twin(zz, way, step, dc):
+        return remote(
+            rows_at(zz), rows_at(zz), w_send.at[way, step, dc], w_recv.at[way, step, dc],
+            place(dc=dc),
+        )
+
+    chained = []
+
+    def when(wanted, copy):
+        @pl.when(wanted)
+        def _():
+            copy.start()
+
+        chained.append((wanted, copy))
+
+    def can_go(way):
+        return z > 0 if way else z < along - 1
+
+    for way in range(2):
+        when(can_go(way), pass_line(z, way, 0))
     for dc in range(1, cores):
-        launch(pass_rows(0, dc, False))
-    if not column:
-        relay_block(1, 0)
-    for dz in beyond:
+        launch(pass_twin(z, 0, 0, dc))
+
+    def follow(step):
+        for way in range(2):
+            zz = z + step if way else z - step
+            there = zz < along if way else zz >= 0
+
+            @pl.when(there)
+            def _(way=way, zz=zz):
+                pass_line(zz, way, step - 1).wait_recv()
+
+            if step < along - 1:
+                when(jnp.logical_and(there, can_go(way)), pass_line(zz, way, step))
+            for dc in range(1, cores):
+                when(there, pass_twin(zz, way, step, dc))
+
+    send_column(1, far_first[1:])
+    for dz in far_first[1:2]:
+        spread_block(0, dz, x_too=False)
+    for dz in far_first[2:]:
+        spread_block(0, dz)
+    for dz in far_first[1:]:
+        relay_block(0, dz)
+    for step in beyond:
+        follow(step)
+    for dz in far_first[:1]:
         spread_block(1, dz)
-    for dz in range(1, along):
-        pass_rows(dz, 0, False).wait_recv()
-        for dc in range(1, cores):
-            launch(pass_rows(dz, dc, True))
-    finish_weights(0)
-    for dz in range(along):
-        for dc in range(1, cores):
-            pass_rows(dz, dc, dz > 0).wait_recv()
+    for dz in everywhere:
+        finish_block(0, dz)
+    for dc in range(1, cores):
+        pass_twin(z, 0, 0, dc).wait_recv()
+        for step in beyond:
+            for way in range(2):
+                zz = z + step if way else z - step
+
+                @pl.when(zz < along if way else zz >= 0)
+                def _(way=way, zz=zz, step=step, dc=dc):
+                    pass_twin(zz, way, step, dc).wait_recv()
 
     def climb(i):
         product = jnp.dot(normed_all[...], up_buf[i], preferred_element_type=F32)
@@ -609,26 +703,22 @@
         hidden[:, cols] = jnp.square(jnp.maximum(product, 0.0)).astype(BF16)
 
     each(0, peers, climb)
-    for dz in beyond:
-        relay_block(1, dz)
-    finish_weights(1)
-
     own = along * rows
-    chunks = 4
-    width = model // chunks
-    per = width // depth
+    strip = model // along
+
+    def strip_of(dz):
+        start = turn(z, along - dz, along) * strip
+        return pl.ds(pl.multiple_of(start, strip), strip)
 
     def halves(k, dc):
-        cols = pl.ds(k * width, width)
         return remote(
-            half_out.at[dc - 1, :, cols], half_in.at[dc - 1, :, cols],
+            half_out.at[dc - 1, :, strip_of(k)], half_in.at[dc - 1, :, strip_of(k)],
             h_send.at[k, dc - 1], h_recv.at[k, dc - 1], place(dc=dc),
         )
 
     def sums(k, dz):
-        cols = pl.ds(k * width, width)
         return remote(
-            rows_out.at[dz - 1, :, cols], rows_in.at[dz - 1, :, cols],
+            rows_out.at[dz - 1, :, strip_of(k)], rows_in.at[dz - 1, :, strip_of(k)],
             r_send.at[k, dz - 1], r_recv.at[k, dz - 1], place(dz=dz),
         )
 
@@ -640,41 +730,61 @@
         return found
 
     def descend(k):
-        def one(s):
-            cols = pl.ds(pl.multiple_of((k * per + s) * depth, depth), depth)
+        finish_block(1, k)
+
+        def one(i):
+            shard = origin(k) - x + i
+            cols = pl.ds(pl.multiple_of(shard * depth, depth), depth)
             channel[:, cols] = jnp.dot(
-                hidden[...], down_buf[k * per + s], preferred_element_type=F32
+                hidden[...], down_buf[shard], preferred_element_type=F32
             )
 
-        each(0, per, one)
-        cols = pl.ds(k * width, width)
+        each(0, across, one)
+        cols = strip_of(k)
         for dc in range(1, cores):
             theirs = pl.ds(pl.multiple_of(turn(c, dc, cores) * own, own), own)
             half_out[dc - 1, :, cols] = channel[theirs, cols].astype(BF16)
             launch(halves(k, dc))
 
     def hand_on(k):
-        cols = pl.ds(k * width, width)
+        cols = strip_of(k)
         for dc in range(1, cores):
             halves(k, dc).wait_recv()
-        for dz in range(1, along):
+        for dz in far_first:
             rows_out[dz - 1, :, cols] = gathered(turn(z, dz, along), cols).astype(BF16)
             launch(sums(k, dz))
 
-    for k in range(chunks):
-        descend(k)
-        if k:
-            hand_on(k - 1)
-    hand_on(chunks - 1)
-    for k in range(chunks):
-        cols = pl.ds(k * width, width)
+    descend(0)
+    for dz in far_first[:1]:
+        relay_block(1, dz)
+    hand_on(0)
+    for dz in far_first[1:]:
+        spread_block(1, dz)
+    last = 0
+    for dz in far_first:
+        if dz not in far_first[:1]:
+            relay_block(1, dz)
+        descend(dz)
+        if last:
+            hand_on(last)
+        last = dz
+    hand_on(last)
+    for k in everywhere:
+        for dz in range(1, along):
+            sums(k, dz).wait_recv()
+    for k in everywhere:
+        cols = pl.ds(k * strip, strip)
         total = updated[:, cols] + gathered(z, cols)
         for dz in range(1, along):
-            sums(k, dz).wait_recv()
             total = total + rows_in[dz - 1, :, cols].astype(F32)
         o_ref[:, cols] = total.astype(BF16)
 
     drain()
+    for wanted, copy in chained:
+        @pl.when(wanted)
+        def _(copy=copy):
+            copy.wait_send()
+
     for copy in started:
         copy.wait_send()
 
@@ -711,7 +821,7 @@
     dma = pltpu.SemaphoreType.DMA
     if column:
         span = 2 * tok + pad
-        in_specs = [anywhere] * 6 + [vmem] * 6 + [anywhere] * 2
+        in_specs = [anywhere] * 6 + [vmem] * 3 + [anywhere] * 2 + [vmem] + [anywhere] * 2
         attention_scratch = [
             pltpu.VMEM((parts, 2, span, part_columns), BF16),
             pltpu.VMEM((parts, 2, tok, part_columns), BF16),
@@ -733,7 +843,7 @@
             dma((parts, 2)),
         ]
     else:
-        in_specs = [vmem] * 2 + [anywhere] * 6 + [vmem] * 4 + [anywhere] * 2
+        in_specs = [vmem] * 2 + [anywhere] * 6 + [vmem] + [anywhere] * 2 + [vmem] + [anywhere] * 2
         attention_scratch = [
             pltpu.VMEM((2, shards, 2 * tok, columns), BF16),
             pltpu.VMEM((2, shards, pad, tok), BF16),
@@ -750,9 +860,13 @@
             pltpu.VMEM((wide, depth), BF16),
             pltpu.VMEM((peers, model, unit), BF16),
             pltpu.VMEM((shards, peers * unit, depth), BF16),
+            pltpu.VMEM((2 * columns, model), BF16),
             pltpu.VMEM((tok, 2 * columns), BF16),
-            pltpu.VMEM((tok, model), BF16),
-            pltpu.VMEM((peers - 1, rows, model), BF16),
+            pltpu.VMEM((tok, model), F32),
+            pltpu.VMEM((cores - 1, lanes * rows, model), BF16),
+            pltpu.VMEM((cores - 1, lanes * rows, model), BF16),
+            pltpu.VMEM((lanes - 1, rows, model), BF16),
+            pltpu.VMEM((lanes - 1, rows, model), BF16),
             pltpu.VMEM((rows, model), F32),
             pltpu.VMEM((group * rows, model), BF16),
             pltpu.VMEM((group * rows, peers * unit), BF16),
@@ -763,18 +877,22 @@
             pltpu.VMEM((along - 1, rows, model), BF16),
             dma((2, along, cores)),
             dma((2, along, cores)),
-            dma((2, along, lanes, across)),
-            dma((2, along, across, lanes)),
-            dma((2, along, across, lanes)),
-            dma((peers - 1,)),
-            dma((peers - 1,)),
+            dma((2, along, cores, lanes, across)),
+            dma((2, along, cores, across, lanes)),
+            dma((2, along, cores, across, lanes)),
+            dma((chunks, cores)),
+            dma((chunks, cores)),
+            dma((chunks, lanes)),
+            dma((chunks, lanes)),
+            dma((2, along)),
+            dma((2, along)),
+            dma((2, along, cores)),
+            dma((2, along, cores)),
             dma((along, cores)),
             dma((along, cores)),
-            dma((chunks, cores)),
-            dma((chunks, cores)),
-            dma((chunks, along)),
-            dma((chunks, along)),
-            dma((group + 3,)),
+            dma((along, along)),
+            dma((along, along)),
+            dma((group + 5,)),
             dma((6 * max(parts, 1),)),
         ] + attention_scratch,
         compiler_params=pltpu.CompilerParams(

time: 155 us -> 143 us (0.923)
  Pallas kernels: 153 us -> 141 us
    pallas_call x1, Pallas kernels: 153 us -> 141 us  [local(): pl.pallas_call(functools.partial(kernel, shards, peers, order, across, co...]
where the time goes in v3:
time: 143 us
  Pallas kernels  141 us (99%)
  local copies, waits for them, and re-layouts  1.67 us (1%)
    pallas_call x1, Pallas kernels, local(): pl.pallas_call(functools.partial(kernel, shards, peers, order, across, co...  141 us

profile of v3, /device:TPU:0, one launch (start us, length us, event | category | flops | bytes accessed | tf_op | source)
XLA Modules:
  0.0 143.0 jit_solution(2497273010772078856)
XLA Ops:
  0.0 141.3 %shard_map.136 = bf16[64,2048]{1,0:T(8,128)(2,1)} custom-call(bf16[256,256]{1,0:T(8,128)(2,1)} %q_n.1, bf16[256,256]{1,0:T(8,128)(2,1)} %q_b.1, bf16[256,256]{1,0:T(8,128)(2,1)} %k_n.1, bf16[256,256]{1,0:T(8,128)(2,1)} %v_n.1, bf16[256,256]{1,0:T(8,128)(2,1)} %k_b.1, bf16[256,256]{1,0:T(8,128)(2,1)} %v_b.1, bf16[4,256]{1,0:T(4,128)(2,1)} %off_n.1, ...), custom_call_target="tpu_custom_call" | custom-call | tf_op jit(solution)/shard_map/pallas_call | solution.py:853
  141.3 1.7 %copy.16 = bf16[64,2048]{1,0:T(8,128)(2,1)} copy(bf16[64,2048]{1,0:T(8,128)(2,1)} %shard_map.136) | data formatting | bytes 524288

commit v4 on v3

--- a/solution.py
+++ b/solution.py
@@ -623,7 +623,7 @@
     scale = lax.rsqrt(jnp.mean(value * value, axis=-1, keepdims=True) + 1e-06)
 
     def rows_of(zz, cc):
-        return pl.ds(pl.multiple_of((cc * along + zz) * rows, rows), rows)
+        return pl.ds(pl.multiple_of((zz * cores + cc) * rows, rows), rows)
 
     normed_all[rows_of(z, c), :] = (value * scale * gain[...]).astype(BF16)
 
@@ -674,36 +674,64 @@
             for dc in range(1, cores):
                 when(there, pass_twin(zz, way, step, dc))
 
-    send_column(1, far_first[1:])
     for dz in far_first[1:2]:
         spread_block(0, dz, x_too=False)
     for dz in far_first[2:]:
         spread_block(0, dz)
+    def climb(zz):
+        slab = pl.ds(pl.multiple_of(zz * cores * rows, cores * rows), cores * rows)
+
+        def one(i):
+            product = jnp.dot(normed_all[slab, :], up_buf[i], preferred_element_type=F32)
+            cols = pl.ds(pl.multiple_of(i * unit, unit), unit)
+            hidden[slab, cols] = jnp.square(jnp.maximum(product, 0.0)).astype(BF16)
+
+        each(0, peers, one)
+
+    def climb_step(step):
+        def side(way):
+            zz = jnp.where(way == 1, z + step, z - step)
+
+            @pl.when(jnp.logical_and(zz >= 0, zz < along))
+            def _():
+                for dc in range(1, cores):
+                    pass_twin(zz, way, step, dc).wait_recv()
+                climb(zz)
+
+        each(0, 2, side)
+
+    def pass_on(step):
+        follow(step)
+        send_column(1, far_first[step : step + 1])
+
+    pass_on(1)
     for dz in far_first[1:]:
         relay_block(0, dz)
-    for step in beyond:
-        follow(step)
     for dz in far_first[:1]:
         spread_block(1, dz)
+    for step in beyond[1:-1]:
+        pass_on(step)
+    for dz in far_first[1:2]:
+        spread_block(1, dz)
+    for dz in far_first[:1]:
+        relay_block(1, dz)
     for dz in everywhere:
         finish_block(0, dz)
     for dc in range(1, cores):
         pass_twin(z, 0, 0, dc).wait_recv()
-        for step in beyond:
-            for way in range(2):
-                zz = z + step if way else z - step
-
-                @pl.when(zz < along if way else zz >= 0)
-                def _(way=way, zz=zz, step=step, dc=dc):
-                    pass_twin(zz, way, step, dc).wait_recv()
-
-    def climb(i):
-        product = jnp.dot(normed_all[...], up_buf[i], preferred_element_type=F32)
-        cols = pl.ds(pl.multiple_of(i * unit, unit), unit)
-        hidden[:, cols] = jnp.square(jnp.maximum(product, 0.0)).astype(BF16)
-
-    each(0, peers, climb)
-    own = along * rows
+    climb(z)
+    climb_step(1)
+    for step in beyond[1:-1]:
+        climb_step(step)
+    for step in beyond[1:][-1:]:
+        pass_on(step)
+    for dz in far_first[1:2]:
+        relay_block(1, dz)
+    for dz in far_first[2:]:
+        spread_block(1, dz)
+    for step in beyond[1:][-1:]:
+        climb_step(step)
+
     strip = model // along
 
     def strip_of(dz):
@@ -742,8 +770,10 @@
         each(0, across, one)
         cols = strip_of(k)
         for dc in range(1, cores):
-            theirs = pl.ds(pl.multiple_of(turn(c, dc, cores) * own, own), own)
-            half_out[dc - 1, :, cols] = channel[theirs, cols].astype(BF16)
+            for zz in everywhere:
+                half_out[dc - 1, pl.ds(zz * rows, rows), cols] = channel[
+                    rows_of(zz, turn(c, dc, cores)), cols
+                ].astype(BF16)
             launch(halves(k, dc))
 
     def hand_on(k):
@@ -755,18 +785,12 @@
             launch(sums(k, dz))
 
     descend(0)
-    for dz in far_first[:1]:
-        relay_block(1, dz)
-    hand_on(0)
-    for dz in far_first[1:]:
-        spread_block(1, dz)
     last = 0
-    for dz in far_first:
-        if dz not in far_first[:1]:
+    for i, dz in enumerate(far_first):
+        if i > 1:
             relay_block(1, dz)
         descend(dz)
-        if last:
-            hand_on(last)
+        hand_on(last)
         last = dz
     hand_on(last)
     for k in everywhere:

time: 143 us -> 128 us (0.90)
  Pallas kernels: 141 us -> 126 us
    pallas_call x1, Pallas kernels: 141 us -> 126 us  [local(): pl.pallas_call(functools.partial(kernel, shards, peers, order, across, co...]
where the time goes in v4:
time: 128 us
  Pallas kernels  126 us (98%)
  local copies, waits for them, and re-layouts  1.67 us (1%)
    pallas_call x1, Pallas kernels, local(): pl.pallas_call(functools.partial(kernel, shards, peers, order, across, co...  126 us

profile of v4, /device:TPU:0, one launch (start us, length us, event | category | flops | bytes accessed | tf_op | source)
XLA Modules:
  0.0 127.6 jit_solution(7779573116041900373)
XLA Ops:
  0.0 126.0 %shard_map.136 = bf16[64,2048]{1,0:T(8,128)(2,1)} custom-call(bf16[256,256]{1,0:T(8,128)(2,1)} %q_n.1, bf16[256,256]{1,0:T(8,128)(2,1)} %q_b.1, bf16[256,256]{1,0:T(8,128)(2,1)} %k_n.1, bf16[256,256]{1,0:T(8,128)(2,1)} %v_n.1, bf16[256,256]{1,0:T(8,128)(2,1)} %k_b.1, bf16[256,256]{1,0:T(8,128)(2,1)} %v_b.1, bf16[4,256]{1,0:T(4,128)(2,1)} %off_n.1, ...), custom_call_target="tpu_custom_call" | custom-call | tf_op jit(solution)/shard_map/pallas_call | solution.py:877
  126.0 1.7 %copy.16 = bf16[64,2048]{1,0:T(8,128)(2,1)} copy(bf16[64,2048]{1,0:T(8,128)(2,1)} %shard_map.136) | data formatting | bytes 524288

commit v5 on v4

--- a/solution.py
+++ b/solution.py
@@ -678,27 +678,102 @@
         spread_block(0, dz, x_too=False)
     for dz in far_first[2:]:
         spread_block(0, dz)
+    strip = model // along
+
+    def strip_of(dz):
+        start = turn(z, along - dz, along) * strip
+        return pl.ds(pl.multiple_of(start, strip), strip)
+
+    def group_rows(zz):
+        return pl.ds(pl.multiple_of(zz * rows, rows), rows)
+
+    def halves(k, zz, dc):
+        return remote(
+            half_out.at[dc - 1, group_rows(zz), strip_of(k)],
+            half_in.at[dc - 1, group_rows(zz), strip_of(k)],
+            h_send.at[k, zz, dc - 1], h_recv.at[k, zz, dc - 1], place(dc=dc),
+        )
+
+    def sums(k, dz):
+        return remote(
+            rows_out.at[dz - 1, :, strip_of(k)], rows_in.at[dz - 1, :, strip_of(k)],
+            r_send.at[k, dz - 1], r_recv.at[k, dz - 1], place(dz=dz),
+        )
+
+    def gathered(zz, cols):
+        found = channel[rows_of(zz, c), cols]
+        at = pl.ds(pl.multiple_of(zz * rows, rows), rows)
+        for dc in range(1, cores):
+            found = found + half_in[dc - 1, at, cols].astype(F32)
+        return found
+
+    def share_rows(k, zz):
+        for dc in range(1, cores):
+            half_out[dc - 1, group_rows(zz), strip_of(k)] = channel[
+                rows_of(zz, turn(c, dc, cores)), strip_of(k)
+            ].astype(BF16)
+            halves(k, zz, dc).start()
+
+    def hand_rows(k, dz):
+        zz = turn(z, dz, along)
+        for dc in range(1, cores):
+            halves(k, zz, dc).wait_recv()
+        rows_out[dz - 1, :, strip_of(k)] = gathered(zz, strip_of(k)).astype(BF16)
+        sums(k, dz).start()
+
+    def slab(zz):
+        return pl.ds(pl.multiple_of(zz * cores * rows, cores * rows), cores * rows)
+
+    def descend_rows(k, zz):
+        def one(i):
+            shard = origin(k) - x + i
+            cols = pl.ds(pl.multiple_of(shard * depth, depth), depth)
+            channel[slab(zz), cols] = jnp.dot(
+                hidden[slab(zz), :], down_buf[shard], preferred_element_type=F32
+            )
+
+        each(0, across, one)
+        share_rows(k, zz)
+
     def climb(zz):
-        slab = pl.ds(pl.multiple_of(zz * cores * rows, cores * rows), cores * rows)
-
         def one(i):
-            product = jnp.dot(normed_all[slab, :], up_buf[i], preferred_element_type=F32)
+            product = jnp.dot(
+                normed_all[slab(zz), :], up_buf[i], preferred_element_type=F32
+            )
             cols = pl.ds(pl.multiple_of(i * unit, unit), unit)
-            hidden[slab, cols] = jnp.square(jnp.maximum(product, 0.0)).astype(BF16)
+            hidden[slab(zz), cols] = jnp.square(jnp.maximum(product, 0.0)).astype(BF16)
 
         each(0, peers, one)
 
-    def climb_step(step):
+    def sides(step, body):
         def side(way):
             zz = jnp.where(way == 1, z + step, z - step)
 
             @pl.when(jnp.logical_and(zz >= 0, zz < along))
             def _():
-                for dc in range(1, cores):
-                    pass_twin(zz, way, step, dc).wait_recv()
-                climb(zz)
+                body(way, zz)
 
         each(0, 2, side)
+
+    early = [0]
+    final_step = max(beyond)
+
+    def work(step):
+        def body(way, zz):
+            for dc in range(1, cores):
+                pass_twin(zz, way, step, dc).wait_recv()
+            climb(zz)
+            for k in early:
+                descend_rows(k, zz)
+
+        sides(step, body)
+
+    def hand(step):
+        def body(way, zz):
+            for k in early:
+                hand_rows(k, turn(zz, along - z, along))
+
+        sides(step, body)
 
     def pass_on(step):
         follow(step)
@@ -717,45 +792,27 @@
         relay_block(1, dz)
     for dz in everywhere:
         finish_block(0, dz)
-    for dc in range(1, cores):
-        pass_twin(z, 0, 0, dc).wait_recv()
-    climb(z)
-    climb_step(1)
-    for step in beyond[1:-1]:
-        climb_step(step)
-    for step in beyond[1:][-1:]:
-        pass_on(step)
+    for k in early:
+        finish_block(1, k)
+    for step in beyond[:-1]:
+        work(step)
+        if step > 1:
+            hand(step - 1)
+    for step in beyond[:-1][-1:]:
+        hand(step)
+    if final_step > 1:
+        pass_on(final_step)
     for dz in far_first[1:2]:
         relay_block(1, dz)
     for dz in far_first[2:]:
         spread_block(1, dz)
-    for step in beyond[1:][-1:]:
-        climb_step(step)
-
-    strip = model // along
-
-    def strip_of(dz):
-        start = turn(z, along - dz, along) * strip
-        return pl.ds(pl.multiple_of(start, strip), strip)
-
-    def halves(k, dc):
-        return remote(
-            half_out.at[dc - 1, :, strip_of(k)], half_in.at[dc - 1, :, strip_of(k)],
-            h_send.at[k, dc - 1], h_recv.at[k, dc - 1], place(dc=dc),
-        )
-
-    def sums(k, dz):
-        return remote(
-            rows_out.at[dz - 1, :, strip_of(k)], rows_in.at[dz - 1, :, strip_of(k)],
-            r_send.at[k, dz - 1], r_recv.at[k, dz - 1], place(dz=dz),
-        )
-
-    def gathered(zz, cols):
-        found = channel[rows_of(zz, c), cols]
-        at = pl.ds(pl.multiple_of(zz * rows, rows), rows)
-        for dc in range(1, cores):
-            found = found + half_in[dc - 1, at, cols].astype(F32)
-        return found
+    work(final_step)
+    for dc in range(1, cores):
+        pass_twin(z, 0, 0, dc).wait_recv()
+    climb(z)
+    for k in early:
+        descend_rows(k, z)
+    hand(final_step)
 
     def descend(k):
         finish_block(1, k)
@@ -768,31 +825,18 @@
             )
 
         each(0, across, one)
-        cols = strip_of(k)
+        for zz in everywhere:
+            share_rows(k, zz)
+
+    for i, k in enumerate(far_first):
+        descend(k)
+        if i == len(far_first) - 2:
+            relay_block(1, far_first[-1])
+        for dz in far_first:
+            hand_rows(k, dz)
+    for k in everywhere:
         for dc in range(1, cores):
-            for zz in everywhere:
-                half_out[dc - 1, pl.ds(zz * rows, rows), cols] = channel[
-                    rows_of(zz, turn(c, dc, cores)), cols
-                ].astype(BF16)
-            launch(halves(k, dc))
-
-    def hand_on(k):
-        cols = strip_of(k)
-        for dc in range(1, cores):
-            halves(k, dc).wait_recv()
-        for dz in far_first:
-            rows_out[dz - 1, :, cols] = gathered(turn(z, dz, along), cols).astype(BF16)
-            launch(sums(k, dz))
-
-    descend(0)
-    last = 0
-    for i, dz in enumerate(far_first):
-        if i > 1:
-            relay_block(1, dz)
-        descend(dz)
-        hand_on(last)
-        last = dz
-    hand_on(last)
+            halves(k, z, dc).wait_recv()
     for k in everywhere:
         for dz in range(1, along):
             sums(k, dz).wait_recv()
@@ -804,6 +848,12 @@
         o_ref[:, cols] = total.astype(BF16)
 
     drain()
+    for k in everywhere:
+        for dz in beyond:
+            sums(k, dz).wait_send()
+        for zz in everywhere:
+            for dc in range(1, cores):
+                halves(k, zz, dc).wait_send()
     for wanted, copy in chained:
         @pl.when(wanted)
         def _(copy=copy):
@@ -912,8 +962,8 @@
             dma((2, along)),
             dma((2, along, cores)),
             dma((2, along, cores)),
-            dma((along, cores)),
-            dma((along, cores)),
+            dma((along, along, cores)),
+            dma((along, along, cores)),
             dma((along, along)),
             dma((along, along)),
             dma((group + 5,)),

time: 128 us -> 126 us (0.984)
  Pallas kernels: 126 us -> 124 us
    pallas_call x1, Pallas kernels: 126 us -> 124 us  [local(): pl.pallas_call(functools.partial(kernel, shards, peers, order, across, co...]
where the time goes in v5:
time: 126 us
  Pallas kernels  124 us (98%)
  local copies, waits for them, and re-layouts  1.67 us (1%)
    pallas_call x1, Pallas kernels, local(): pl.pallas_call(functools.partial(kernel, shards, peers, order, across, co...  124 us

profile of v5, /device:TPU:0, one launch (start us, length us, event | category | flops | bytes accessed | tf_op | source)
XLA Modules:
  0.0 126.0 jit_solution(1782736389406273100)
XLA Ops:
  0.0 124.3 %shard_map.136 = bf16[64,2048]{1,0:T(8,128)(2,1)} custom-call(bf16[256,256]{1,0:T(8,128)(2,1)} %q_n.1, bf16[256,256]{1,0:T(8,128)(2,1)} %q_b.1, bf16[256,256]{1,0:T(8,128)(2,1)} %k_n.1, bf16[256,256]{1,0:T(8,128)(2,1)} %v_n.1, bf16[256,256]{1,0:T(8,128)(2,1)} %k_b.1, bf16[256,256]{1,0:T(8,128)(2,1)} %v_b.1, bf16[4,256]{1,0:T(4,128)(2,1)} %off_n.1, ...), custom_call_target="tpu_custom_call" | custom-call | tf_op jit(solution)/shard_map/pallas_call | solution.py:927
  124.3 1.7 %copy.16 = bf16[64,2048]{1,0:T(8,128)(2,1)} copy(bf16[64,2048]{1,0:T(8,128)(2,1)} %shard_map.136) | data formatting | bytes 524288

commit v6 on v5

--- a/solution.py
+++ b/solution.py
@@ -832,7 +832,7 @@
         descend(k)
         if i == len(far_first) - 2:
             relay_block(1, far_first[-1])
-        for dz in far_first:
+        for dz in far_first[1:] + far_first[:1]:
             hand_rows(k, dz)
     for k in everywhere:
         for dc in range(1, cores):

time: 126 us -> 125 us (level)
  no operation moved by 1% of the time
where the time goes in v6:
time: 125 us
  Pallas kernels  123 us (98%)
  local copies, waits for them, and re-layouts  1.67 us (1%)
    pallas_call x1, Pallas kernels, local(): pl.pallas_call(functools.partial(kernel, shards, peers, order, across, co...  123 us

profile of v6, /device:TPU:0, one launch (start us, length us, event | category | flops | bytes accessed | tf_op | source)
XLA Modules:
  0.0 125.1 jit_solution(9255202358750427776)
XLA Ops:
  0.0 123.4 %shard_map.136 = bf16[64,2048]{1,0:T(8,128)(2,1)} custom-call(bf16[256,256]{1,0:T(8,128)(2,1)} %q_n.1, bf16[256,256]{1,0:T(8,128)(2,1)} %q_b.1, bf16[256,256]{1,0:T(8,128)(2,1)} %k_n.1, bf16[256,256]{1,0:T(8,128)(2,1)} %v_n.1, bf16[256,256]{1,0:T(8,128)(2,1)} %k_b.1, bf16[256,256]{1,0:T(8,128)(2,1)} %v_b.1, bf16[4,256]{1,0:T(4,128)(2,1)} %off_n.1, ...), custom_call_target="tpu_custom_call" | custom-call | tf_op jit(solution)/shard_map/pallas_call | solution.py:927
  123.4 1.7 %copy.16 = bf16[64,2048]{1,0:T(8,128)(2,1)} copy(bf16[64,2048]{1,0:T(8,128)(2,1)} %shard_map.136) | data formatting | bytes 524288
